TPU v7x, 256 devices: a whole 4x4x8 slice. The times are simulated.
256 devices in a mesh: ep: 32 (over z, x), tp: 8 (over y, core).
Axes of the slice: x: 4, y: 4, z: 8, core: 2. Of those that a mesh axis runs over, the one named last changes fastest.
Arguments:
- hidden_in: bfloat16 [1024, 2048], P('ep', 'tp'), may hold values from -6 to 6
- state_in: float32 [1024, 8, 128, 128], P('ep', 'tp'), may hold values from -0.6 to 0.6
- attn_gain: float32 [2048], replicated, may hold values from 0.1 to 1.9
- w_query: bfloat16 [2048, 1024], P(None, 'tp'), may hold values from -0.125 to 0.125
- w_key: bfloat16 [2048, 1024], P(None, 'tp'), may hold values from -0.125 to 0.125
- w_value: bfloat16 [2048, 1024], P(None, 'tp'), may hold values from -0.125 to 0.125
- w_gate: bfloat16 [2048, 1024], P(None, 'tp'), may hold values from -0.125 to 0.125
- w_beta: bfloat16 [2048, 8], replicated, may hold values from -0.125 to 0.125
- w_decay: bfloat16 [2048, 8], replicated, may hold values from -0.125 to 0.125
- decay_scale: float32 [8], replicated, may hold values from 0.05 to 3
- head_gain: float32 [128], replicated, may hold values from 0.1 to 1.9
- w_output: bfloat16 [1024, 2048], P(None, 'tp'), may hold values from -0.1875 to 0.1875
- ffn_gain: float32 [2048], replicated, may hold values from 0.1 to 1.9
- expert_ids: int32 [1024, 2], P('ep'), may hold values from 0 to 31, all different within a row; in each aligned block of 32 rows (0 to 31, 32 to 63, ...) at most 4 rows name the same one
- route_weight: float32 [1024, 2], P('ep'), may hold values from 0.2 to 1
- expert_gate: bfloat16 [32, 2048, 3072], P('ep', None, 'tp'), may hold values from -0.125 to 0.125
- expert_up: bfloat16 [32, 2048, 3072], P('ep', None, 'tp'), may hold values from -0.125 to 0.125
- expert_down: bfloat16 [32, 3072, 2048], P('ep', 'tp'), may hold values from -0.109375 to 0.109375
- dense_gate: bfloat16 [2048, 4096], P(None, 'ep'), may hold values from -0.125 to 0.125
- dense_up: bfloat16 [2048, 4096], P(None, 'ep'), may hold values from -0.125 to 0.125
- dense_down: bfloat16 [4096, 2048], P('ep'), may hold values from -0.09375 to 0.09375
- dense_mix: float32 [2048], P('tp'), may hold values from -6 to 6
Outputs:
- result: bfloat16 [1024, 2048], P('ep', 'tp')
- new_state: float32 [1024, 8, 128, 128], P('ep', 'tp')
Inputs may be any that keep to these rules, and one draw needn't show every extreme that they name: `expert_ids`: each row names 2 different experts. Within the rows of one index of ep (aligned blocks of 32 sequences) no expert is named more than 4 times, a bound that some block reaches.
All inputs are finite; a program needn't handle non-finite values.
Results may differ from a plain program's by a relative error of at most 0.015.
Values may be sent and summed in bfloat16 or wider, within the bound.
A program may use at most 64 MiB of HBM per device.

v0:
```python
import jax
import jax.numpy as jnp
from jax import lax
from jax.sharding import Mesh
from jax.sharding import PartitionSpec as P

EP = ("ep_0", "ep_1")


EPS = 1e-06


def sent_to_all(array, axis):
    copies = jnp.broadcast_to(array, (lax.axis_size(axis), *array.shape))
    return lax.all_to_all(copies, axis, split_axis=0, concat_axis=0, tiled=True)


def in_order(blocks, dim):
    blocks = jnp.moveaxis(blocks, 0, dim)
    shape = blocks.shape
    return blocks.reshape(*shape[:dim], shape[dim] * shape[dim + 1], *shape[dim + 2 :])


def collect(array, axis, dim):
    blocks = sent_to_all(array, axis)
    return in_order(blocks, dim)


def split_up(array, dim, length):
    before, after = (array.shape[:dim], array.shape[dim + 1 :])
    return jnp.moveaxis(array.reshape(*before, length, -1, *after), dim, 0)


def sum_at_owner(array, axis, dim):
    length = lax.axis_size(axis)
    blocks = lax.all_to_all(split_up(array, dim, length), axis, 0, 0, tiled=True)
    return jnp.sum(blocks.astype(jnp.float32), axis=0)


def gathered_by_axis(array, axes, dim):
    for axis in reversed(axes):
        array = lax.all_gather(array, axis, axis=dim, tiled=True)
    return array


def root_norm(values, scale_vec):
    wide = values.astype(jnp.float32)
    return wide * lax.rsqrt(jnp.mean(wide * wide, axis=-1, keepdims=True) + EPS) * scale_vec


def unit_norm(values):
    return values * lax.rsqrt(jnp.sum(values * values, axis=-1, keepdims=True) + EPS)


def slot_table(expert_ids, count):
    flat = expert_ids.reshape(-1)
    onehot = (flat[:, None] == jnp.arange(count, dtype=jnp.int32)[None, :]).astype(jnp.int32)
    before = jnp.cumsum(onehot, axis=0) - onehot
    return jnp.sum(before * onehot, axis=1).reshape(expert_ids.shape)


def delta_update(old_state, key_rows, value_rows, beta_rate, decay_rate):
    recalled = jnp.einsum("shk,shkv->shv", key_rows, old_state)
    erased = (
        old_state - beta_rate[..., None, None] * key_rows[..., :, None] * recalled[..., None, :]
    )
    written = beta_rate[..., None, None] * key_rows[..., :, None] * value_rows[..., None, :]
    return decay_rate[..., None, None] * erased + written


def head_output(new_state, queries, gate_rows, head_gain):
    read = jnp.einsum("shk,shkv->shv", queries, new_state)
    return (root_norm(read, head_gain) * jax.nn.silu(gate_rows)).astype(jnp.bfloat16)


def per_device(
    hidden_in,
    state_in,
    attn_gain,
    w_query,
    w_key,
    w_value,
    w_gate,
    w_beta,
    w_decay,
    decay_scale,
    head_gain,
    w_output,
    ffn_gain,
    expert_ids,
    route_weight,
    expert_gate,
    expert_up,
    expert_down,
    dense_gate,
    dense_up,
    dense_down,
    dense_mix,
):
    seq_dev = hidden_in.shape[0]
    tp_size = lax.axis_size("tp")
    ep_size = lax.axis_size(EP)
    tp_index = lax.axis_index("tp")
    local_heads = state_in.shape[1]
    key_dim = state_in.shape[2]
    value_dim = state_in.shape[3]
    local_width = hidden_in.shape[1]
    model_width = local_width * tp_size
    full_rows = collect(hidden_in, "tp", 1)
    normed = root_norm(full_rows, attn_gain).astype(jnp.bfloat16)
    queries = unit_norm(
        jnp.dot(normed, w_query, preferred_element_type=jnp.float32).reshape(
            seq_dev, local_heads, key_dim
        )
    ) * key_dim ** (-0.5)
    key_rows = unit_norm(
        jnp.dot(normed, w_key, preferred_element_type=jnp.float32).reshape(
            seq_dev, local_heads, key_dim
        )
    )
    value_rows = jnp.dot(normed, w_value, preferred_element_type=jnp.float32).reshape(
        seq_dev, local_heads, value_dim
    )
    gate_rows = jnp.dot(normed, w_gate, preferred_element_type=jnp.float32).reshape(
        seq_dev, local_heads, value_dim
    )
    head_start = tp_index * local_heads
    beta_all = jnp.dot(normed, w_beta, preferred_element_type=jnp.float32)
    decay_all = jnp.dot(normed, w_decay, preferred_element_type=jnp.float32)
    beta_rate = jax.nn.sigmoid(lax.dynamic_slice_in_dim(beta_all, head_start, local_heads, 1))
    decay_logit = lax.dynamic_slice_in_dim(decay_all, head_start, local_heads, 1)
    decay_local = lax.dynamic_slice_in_dim(decay_scale, head_start, local_heads, 0)
    decay_rate = jnp.exp(-decay_local[None, :] * jax.nn.softplus(decay_logit))
    new_state = delta_update(state_in, key_rows, value_rows, beta_rate, decay_rate)
    heads_out = head_output(new_state, queries, gate_rows, head_gain).reshape(
        seq_dev, local_heads * value_dim
    )
    all_heads = collect(heads_out, "tp", 1)
    mixed = (
        hidden_in.astype(jnp.float32)
        + jnp.dot(all_heads, w_output, preferred_element_type=jnp.float32)
    ).astype(jnp.bfloat16)
    block_rows = seq_dev // tp_size
    top_count = expert_ids.shape[1]
    experts_all = expert_gate.shape[0] * ep_size
    capacity = max(2, 2 * seq_dev * top_count // experts_all)
    slots = slot_table(expert_ids, experts_all)
    place = expert_ids * capacity + slots
    columns = jnp.arange(experts_all * capacity, dtype=jnp.int32)
    send_matrix = jnp.sum(
        (place[None, :, :] == columns[:, None, None]).astype(jnp.bfloat16), axis=2
    )
    take_matrix = jnp.sum(
        jnp.where(place[:, :, None] == columns[None, None, :], route_weight[:, :, None], 0.0),
        axis=1,
    )
    mixed_full = collect(mixed, "tp", 1)
    normed2 = root_norm(mixed_full, ffn_gain).astype(jnp.bfloat16)
    dense_rows = lax.dynamic_slice_in_dim(normed2, tp_index * block_rows, block_rows, 0)
    outgoing = jnp.dot(send_matrix, normed2, preferred_element_type=jnp.float32).astype(
        jnp.bfloat16
    )
    outgoing = outgoing.reshape(experts_all, capacity, model_width)
    rows = lax.all_to_all(outgoing, EP, split_axis=0, concat_axis=0, tiled=True)
    flat = rows.reshape(-1, rows.shape[2])
    gate_val = jnp.dot(flat, expert_gate[0], preferred_element_type=jnp.float32)
    up_val = jnp.dot(flat, expert_up[0], preferred_element_type=jnp.float32)
    inner = (jax.nn.silu(gate_val) * up_val).astype(jnp.bfloat16)
    partial_out = jnp.dot(inner, expert_down[0], preferred_element_type=jnp.float32).reshape(
        rows.shape
    )
    summed = sum_at_owner(partial_out.astype(jnp.bfloat16), "tp", 2).astype(jnp.bfloat16)
    returned = lax.all_to_all(summed, EP, split_axis=0, concat_axis=0, tiled=True)
    moe_sum = jnp.dot(take_matrix, returned.reshape(-1, local_width).astype(jnp.float32))
    piece = gathered_by_axis(dense_rows, EP, 0)
    gate_val = jnp.dot(piece, dense_gate, preferred_element_type=jnp.float32)
    up_val = jnp.dot(piece, dense_up, preferred_element_type=jnp.float32)
    dense_hidden = (jax.nn.silu(gate_val) * up_val).astype(jnp.bfloat16)
    dense_own = sum_at_owner(
        jnp.dot(dense_hidden, dense_down, preferred_element_type=jnp.float32).astype(jnp.bfloat16),
        EP,
        0,
    )
    dense_out = lax.all_to_all(
        dense_own.astype(jnp.bfloat16), "tp", split_axis=1, concat_axis=0, tiled=True
    ).astype(dense_own.dtype)
    result = (
        mixed.astype(jnp.float32) + moe_sum + jax.nn.sigmoid(dense_mix)[None, :] * dense_out
    ).astype(jnp.bfloat16)
    return (result, new_state)


def solution(mesh):
    torus = Mesh(mesh.devices.reshape(8, 4, mesh.shape["tp"]), ("ep_0", "ep_1", "tp"))
    return jax.shard_map(
        per_device,
        mesh=torus,
        in_specs=(
            P(EP, "tp"),
            P(EP, "tp", None, None),
            P(),
            P(None, "tp"),
            P(None, "tp"),
            P(None, "tp"),
            P(None, "tp"),
            P(),
            P(),
            P(),
            P(),
            P(None, "tp"),
            P(),
            P(EP, None),
            P(EP, None),
            P(EP, None, "tp"),
            P(EP, None, "tp"),
            P(EP, "tp", None),
            P(None, EP),
            P(None, EP),
            P(EP, None),
            P("tp"),
        ),
        out_specs=(P(EP, "tp"), P(EP, "tp", None, None)),
        check_vma=False,
    )
```

profile of v0, /device:TPU:1, one launch (start us, length us, event | category | flops | bytes accessed | tf_op | source)
XLA Modules:
  0.0 151.4 jit_solution(3124206976896148185)
XLA Ops:
  0.7 1.5 %broadcast_in_dim.14 = bf16[8,32,256]{2,1,0:T(8,128)(2,1)} broadcast(bf16[32,256]{1,0:T(8,128)(2,1)} %param.22), dimensions={1,2} | broadcast | bytes 147456 | tf_op jit(solution)/shard_map/broadcast_in_dim | solution.py:14
  2.2 6.5 %all-to-all-start = ((bf16[8,32,256]{2,1,0:T(8,128)(2,1)}), bf16[8,32,256]{2,1,0:T(8,128)(2,1)S(1)}, u32[]{:S(2)}, u32[]{:S(2)}) async-start(bf16[8,32,256]{2,1,0:T(8,128)(2,1)} %broadcast_in_dim.14), calls=%async_computation | async-start | bytes 262144 | tf_op jit(solution)/shard_map/all_to_all | solution.py:15
  8.7 1.2 dynamic_slice.12
  10.6 0.8 copy.80
  11.6 2.3 %all-to-all-done = bf16[8,32,256]{2,1,0:T(8,128)(2,1)S(1)} async-done(((bf16[8,32,256]{2,1,0:T(8,128)(2,1)}), bf16[8,32,256]{2,1,0:T(8,128)(2,1)S(1)}, u32[]{:S(2)}, u32[]{:S(2)}) %all-to-all-start) | async-done | bytes 131104 | tf_op jit(solution)/shard_map/all_to_all | solution.py:15
  14.0 0.1 fusion.19
  14.2 0.9 multiply_convert_fusion.1
  15.1 0.9 fusion.46
  16.0 0.1 fusion.45
  16.1 0.2 fusion.47
  16.4 0.3 multiply_reduce_fusion.1
  16.7 0.3 multiply_reduce_fusion.2
  17.1 0.4 fusion.39
  17.6 0.9 fusion.41
  18.7 0.2 multiply_convert_fusion.2
  18.9 0.6 broadcast_in_dim.15
  19.6 4.1 %all-to-all-start.1 = ((bf16[8,32,128]{2,1,0:T(8,128)(2,1)}), bf16[8,32,128]{2,1,0:T(8,128)(2,1)S(1)}, u32[]{:S(2)}, u32[]{:S(2)}) async-start(bf16[8,32,128]{2,1,0:T(8,128)(2,1)} %broadcast_in_dim.15), calls=%async_computation.1 | async-start | bytes 131072 | tf_op jit(solution)/shard_map/all_to_all | solution.py:15
  23.7 0.2 select_reduce_fusion.1
  24.1 4.5 %all-to-all-done.1 = bf16[8,32,128]{2,1,0:T(8,128)(2,1)S(1)} async-done(((bf16[8,32,128]{2,1,0:T(8,128)(2,1)}), bf16[8,32,128]{2,1,0:T(8,128)(2,1)S(1)}, u32[]{:S(2)}, u32[]{:S(2)}) %all-to-all-start.1) | async-done | bytes 65568 | tf_op jit(solution)/shard_map/all_to_all | solution.py:15
  28.6 0.2 fusion.18
  28.8 0.7 broadcast_in_dim.18
  29.4 4.1 %all-to-all-start.2 = ((bf16[8,32,256]{2,1,0:T(8,128)(2,1)}), bf16[8,32,256]{2,1,0:T(8,128)(2,1)S(1)}, u32[]{:S(2)}, u32[]{:S(2)}) async-start(bf16[8,32,256]{2,1,0:T(8,128)(2,1)} %broadcast_in_dim.18), calls=%async_computation.2 | async-start | bytes 262144 | tf_op jit(solution)/shard_map/all_to_all | solution.py:15
  33.6 5.2 %all-to-all-done.2 = bf16[8,32,256]{2,1,0:T(8,128)(2,1)S(1)} async-done(((bf16[8,32,256]{2,1,0:T(8,128)(2,1)}), bf16[8,32,256]{2,1,0:T(8,128)(2,1)S(1)}, u32[]{:S(2)}, u32[]{:S(2)}) %all-to-all-start.2) | async-done | bytes 131104 | tf_op jit(solution)/shard_map/all_to_all | solution.py:15
  38.8 0.1 fusion.20
  39.1 0.3 convolution_convert_fusion.2
  39.4 1.0 reshape.175
  40.4 10.5 %all-to-all-start.3 = ((bf16[32,4,2048]{2,1,0:T(4,128)(2,1)}), bf16[32,4,2048]{2,1,0:T(4,128)(2,1)S(1)}, u32[]{:S(2)}, u32[]{:S(2)}) async-start(bf16[32,4,2048]{2,1,0:T(4,128)(2,1)} %reshape.175), calls=%async_computation.3 | async-start | bytes 1048576 | tf_op jit(solution)/shard_map/all_to_all | solution.py:164
  50.9 10.0 %all-gather = bf16[4,4,2048]{2,1,0:T(4,128)(2,1)S(1)} all-gather(bf16[1,4,2048]{2,1,0:T(4,128)(2,1)S(1)} %dynamic-slice_bitcast_fusion), channel_id=1, replica_groups=mesh['ep_0'=8,'ep_1'=4,'tp'=8] {'ep_1'}, dimensions={0}, use_global_device_ids=true | all-gather | bytes 81920 | tf_op jit(solution)/shard_map/all_gather | solution.py:42
  60.9 21.5 %all_gather.7 = bf16[128,2048]{1,0:T(8,128)(2,1)S(1)} all-gather(bf16[16,2048]{1,0:T(8,128)(2,1)S(1)} %reshape.184), channel_id=1, replica_groups=mesh['ep_0'=8,'ep_1'=4,'tp'=8] {'ep_0'}, dimensions={0}, use_global_device_ids=true | all-gather | bytes 589824 | tf_op jit(solution)/shard_map/all_gather | solution.py:42
  82.4 0.3 fusion.48
  82.7 1.7 %convolution_convert_fusion = bf16[128,2048]{1,0:T(8,128)(2,1)S(1)} fusion(bf16[128,2048]{1,0:T(8,128)(2,1)} %param.42, bf16[128,2048]{1,0:T(8,128)(2,1)S(1)} %all_gather.7, bf16[2048,128]{1,0:T(8,128)(2,1)} %param.41, f32[128,128]{1,0:T(8,128)S(1)} %fusion.48), kind=kOutput, calls=%fused_computation | convolution fusion | flops 134578176 | bytes 2162688 | tf_op jit(solution)/shard_map/dot_general | solution.py:180
  84.5 1.0 reshape.179
  85.4 7.9 %all-to-all-start.6 = ((bf16[32,4,2048]{2,1,0:T(4,128)(2,1)}), bf16[32,4,2048]{2,1,0:T(4,128)(2,1)S(1)}, u32[]{:S(2)}, u32[]{:S(2)}) async-start(bf16[32,4,2048]{2,1,0:T(4,128)(2,1)} %reshape.179), calls=%async_computation.6 | async-start | bytes 1048576 | tf_op jit(solution)/shard_map/all_to_all | solution.py:36
  93.5 2.0 %fusion.7 = f32[128,384]{1,0:T(8,128)S(1)} fusion(bf16[128,2048]{1,0:T(8,128)(2,1)S(1)} %reshape.176, bf16[1,2048,384]{2,1,0:T(8,128)(2,1)} %param.37), kind=kOutput, calls=%fused_computation.11 | convolution fusion | flops 201326592 | bytes 2293760 | tf_op jit(solution)/shard_map/dot_general | solution.py:166
  95.5 0.5 fusion.12
  96.0 0.4 convolution_convert_fusion.1
  96.4 0.9 copy.103
  97.3 8.7 %all-to-all-done.6 = bf16[32,4,2048]{2,1,0:T(4,128)(2,1)S(1)} async-done(((bf16[32,4,2048]{2,1,0:T(4,128)(2,1)}), bf16[32,4,2048]{2,1,0:T(4,128)(2,1)S(1)}, u32[]{:S(2)}, u32[]{:S(2)}) %all-to-all-start.6) | async-done | bytes 524320 | tf_op jit(solution)/shard_map/all_to_all | solution.py:36
  106.0 13.4 %all-to-all-start.4 = ((bf16[8,32,4,256]{3,1,2,0:T(8,128)(2,1)}), bf16[8,32,4,256]{3,1,2,0:T(8,128)(2,1)S(1)}, u32[]{:S(2)}, u32[]{:S(2)}) async-start(bf16[8,32,4,256]{3,1,2,0:T(8,128)(2,1)} %bitcast.106), calls=%async_computation.4 | async-start | bytes 1048576 | tf_op jit(solution)/shard_map/all_to_all | solution.py:36
  119.6 0.8 reduce_sum.108
  120.4 8.4 %all-to-all-done.4 = bf16[8,32,4,256]{3,1,2,0:T(8,128)(2,1)S(1)} async-done(((bf16[8,32,4,256]{3,1,2,0:T(8,128)(2,1)}), bf16[8,32,4,256]{3,1,2,0:T(8,128)(2,1)S(1)}, u32[]{:S(2)}, u32[]{:S(2)}) %all-to-all-start.4) | async-done | bytes 524320 | tf_op jit(solution)/shard_map/all_to_all | solution.py:36
  128.8 4.2 %all-to-all-start.7 = ((bf16[4,8,256]{2,0,1:T(4,128)(2,1)}), bf16[4,8,256]{2,0,1:T(4,128)(2,1)S(1)}, u32[]{:S(2)}, u32[]{:S(2)}) async-start(bf16[4,8,256]{2,0,1:T(4,128)(2,1)} %bitcast.22), calls=%async_computation.7 | async-start | bytes 32768 | tf_op jit(solution)/shard_map/all_to_all | solution.py:184
  133.1 2.9 %multiply_add_fusion = f32[32,1,128,128]{3,2,1,0:T(8,128)} fusion(f32[32,1,128,128]{3,2,1,0:T(8,128)} %param.23, f32[32,128]{1,0:T(8,128)S(1)} %fusion.47, f32[32,128]{1,0:T(8,128)S(1)} %bitcast.111, f32[32,128]{1,0:T(8,128)S(1)} %get-tuple-element.2, f32[32]{0:T(128)S(1)} %get-tuple-element.9), kind=kLoop, calls=%fused_computation.7 | loop fusion | flops 2621440 | bytes 4243584 | tf_op jit(solution)/shard_map/add | solution.py:68
  136.1 0.7 copy.86
  136.7 1.0 all-to-all-done.7
  137.7 4.1 %all-to-all-start.5 = ((bf16[32,4,256]{2,1,0:T(4,128)(2,1)}), bf16[32,4,256]{2,1,0:T(4,128)(2,1)S(1)}, u32[]{:S(2)}, u32[]{:S(2)}) async-start(bf16[32,4,256]{2,1,0:T(4,128)(2,1)} %copy.86), calls=%async_computation.5 | async-start | bytes 131072 | tf_op jit(solution)/shard_map/all_to_all | solution.py:173
  141.8 8.8 %all-to-all-done.5 = bf16[32,4,256]{2,1,0:T(4,128)(2,1)S(1)} async-done(((bf16[32,4,256]{2,1,0:T(4,128)(2,1)}), bf16[32,4,256]{2,1,0:T(4,128)(2,1)S(1)}, u32[]{:S(2)}, u32[]{:S(2)}) %all-to-all-start.5) | async-done | bytes 65568 | tf_op jit(solution)/shard_map/all_to_all | solution.py:173
  150.7 0.7 fusion.17
  (64 shorter events, 1.5 us)
Async XLA Ops:
  0.6 95.3 %copy-start = (bf16[1,384,2048]{2,1,0:T(8,128)(2,1)S(1)}, bf16[1,384,2048]{2,1,0:T(8,128)(2,1)}, u32[]{:S(2)}) copy-start(bf16[1,384,2048]{2,1,0:T(8,128)(2,1)} %param.39) | copy-start | bytes 4718596
  0.6 15.3 %copy-start.9 = (bf16[2048,8]{0,1:T(8,128)(2,1)S(1)}, bf16[2048,8]{0,1:T(8,128)(2,1)}, u32[]{:S(2)}) copy-start(bf16[2048,8]{0,1:T(8,128)(2,1)} %param.30) | copy-start | bytes 98308
  0.7 15.5 %copy-start.3 = (bf16[2048,128]{1,0:T(8,128)(2,1)S(1)}, bf16[2048,128]{1,0:T(8,128)(2,1)}, u32[]{:S(2)}) copy-start(bf16[2048,128]{1,0:T(8,128)(2,1)} %param.27) | copy-start | bytes 1572868
  0.7 15.7 %copy-start.4 = (bf16[2048,128]{1,0:T(8,128)(2,1)S(1)}, bf16[2048,128]{1,0:T(8,128)(2,1)}, u32[]{:S(2)}) copy-start(bf16[2048,128]{1,0:T(8,128)(2,1)} %param.26) | copy-start | bytes 1572868
  0.7 16.0 %copy-start.5 = (bf16[2048,128]{1,0:T(8,128)(2,1)S(1)}, bf16[2048,128]{1,0:T(8,128)(2,1)}, u32[]{:S(2)}) copy-start(bf16[2048,128]{1,0:T(8,128)(2,1)} %param.25) | copy-start | bytes 1572868
  2.2 11.7 %all-to-all-start = ((bf16[8,32,256]{2,1,0:T(8,128)(2,1)}), bf16[8,32,256]{2,1,0:T(8,128)(2,1)S(1)}, u32[]{:S(2)}, u32[]{:S(2)}) async-start(bf16[8,32,256]{2,1,0:T(8,128)(2,1)} %broadcast_in_dim.14), calls=%async_computation | async-start | bytes 262144 | tf_op jit(solution)/shard_map/all_to_all | solution.py:15
  14.0 3.1 %copy-start.1 = (f32[32,1,128,128]{3,2,1,0:T(8,128)S(1)}, f32[32,1,128,128]{3,2,1,0:T(8,128)}, u32[]{:S(2)}) copy-start(f32[32,1,128,128]{3,2,1,0:T(8,128)} %param.23) | copy-start | bytes 6291460
  17.1 1.6 %copy-start.6 = (bf16[2048,128]{1,0:T(8,128)(2,1)S(1)}, bf16[2048,128]{1,0:T(8,128)(2,1)}, u32[]{:S(2)}) copy-start(bf16[2048,128]{1,0:T(8,128)(2,1)} %param.28) | copy-start | bytes 1572868
  17.1 1.6 %copy-start.14 = (f32[128]{0:T(128)S(1)}, f32[128]{0:T(128)}, u32[]{:S(2)}) copy-start(f32[128]{0:T(128)} %param.32) | copy-start | bytes 1540
  17.5 11.0 %copy-start.2 = (bf16[1024,256]{1,0:T(8,128)(2,1)S(1)}, bf16[1024,256]{1,0:T(8,128)(2,1)}, u32[]{:S(2)}) copy-start(bf16[1024,256]{1,0:T(8,128)(2,1)} %param.33) | copy-start | bytes 1572868
  17.5 11.0 %copy-start.8 = (bf16[32,256]{1,0:T(8,128)(2,1)S(1)}, bf16[32,256]{1,0:T(8,128)(2,1)}, u32[]{:S(2)}) copy-start(bf16[32,256]{1,0:T(8,128)(2,1)} %param.22) | copy-start | bytes 49156
  17.6 15.9 %copy-start.11 = (s32[32,2]{0,1:T(2,128)S(1)}, s32[32,2]{0,1:T(2,128)}, u32[]{:S(2)}) copy-start(s32[32,2]{0,1:T(2,128)} %param.35) | copy-start | bytes 772
  18.6 20.4 %copy-start.10 = (f32[2048]{0:T(1024)S(1)}, f32[2048]{0:T(1024)}, u32[]{:S(2)}) copy-start(f32[2048]{0:T(1024)} %param.34) | copy-start | bytes 24580
  19.6 9.0 %all-to-all-start.1 = ((bf16[8,32,128]{2,1,0:T(8,128)(2,1)}), bf16[8,32,128]{2,1,0:T(8,128)(2,1)S(1)}, u32[]{:S(2)}, u32[]{:S(2)}) async-start(bf16[8,32,128]{2,1,0:T(8,128)(2,1)} %broadcast_in_dim.15), calls=%async_computation.1 | async-start | bytes 131072 | tf_op jit(solution)/shard_map/all_to_all | solution.py:15
  29.4 9.3 %all-to-all-start.2 = ((bf16[8,32,256]{2,1,0:T(8,128)(2,1)}), bf16[8,32,256]{2,1,0:T(8,128)(2,1)S(1)}, u32[]{:S(2)}, u32[]{:S(2)}) async-start(bf16[8,32,256]{2,1,0:T(8,128)(2,1)} %broadcast_in_dim.18), calls=%async_computation.2 | async-start | bytes 262144 | tf_op jit(solution)/shard_map/all_to_all | solution.py:15
  39.0 43.5 %copy-start.7 = (bf16[2048,128]{1,0:T(8,128)(2,1)S(1)}, bf16[2048,128]{1,0:T(8,128)(2,1)}, u32[]{:S(2)}) copy-start(bf16[2048,128]{1,0:T(8,128)(2,1)} %param.40) | copy-start | bytes 1572868
  40.4 45.1 %all-to-all-start.3 = ((bf16[32,4,2048]{2,1,0:T(4,128)(2,1)}), bf16[32,4,2048]{2,1,0:T(4,128)(2,1)S(1)}, u32[]{:S(2)}, u32[]{:S(2)}) async-start(bf16[32,4,2048]{2,1,0:T(4,128)(2,1)} %reshape.175), calls=%async_computation.3 | async-start | bytes 1048576 | tf_op jit(solution)/shard_map/all_to_all | solution.py:164
  85.4 20.6 %all-to-all-start.6 = ((bf16[32,4,2048]{2,1,0:T(4,128)(2,1)}), bf16[32,4,2048]{2,1,0:T(4,128)(2,1)S(1)}, u32[]{:S(2)}, u32[]{:S(2)}) async-start(bf16[32,4,2048]{2,1,0:T(4,128)(2,1)} %reshape.179), calls=%async_computation.6 | async-start | bytes 1048576 | tf_op jit(solution)/shard_map/all_to_all | solution.py:36
  93.5 2.0 %copy-start.15 = (bf16[1,2048,384]{2,1,0:T(8,128)(2,1)S(1)}, bf16[1,2048,384]{2,1,0:T(8,128)(2,1)}, u32[]{:S(2)}) copy-start(bf16[1,2048,384]{2,1,0:T(8,128)(2,1)} %param.38) | copy-start | bytes 4718596
  96.0 23.5 %copy-start.12 = (f32[32,2]{0,1:T(2,128)S(1)}, f32[32,2]{0,1:T(2,128)}, u32[]{:S(2)}) copy-start(f32[32,2]{0,1:T(2,128)} %param.36) | copy-start | bytes 772
  96.0 23.6 %copy-start.13 = (f32[256]{0:T(256)S(1)}, f32[256]{0:T(256)}, u32[]{:S(2)}) copy-start(f32[256]{0:T(256)} %param.43) | copy-start | bytes 3076
  106.0 22.8 %all-to-all-start.4 = ((bf16[8,32,4,256]{3,1,2,0:T(8,128)(2,1)}), bf16[8,32,4,256]{3,1,2,0:T(8,128)(2,1)S(1)}, u32[]{:S(2)}, u32[]{:S(2)}) async-start(bf16[8,32,4,256]{3,1,2,0:T(8,128)(2,1)} %bitcast.106), calls=%async_computation.4 | async-start | bytes 1048576 | tf_op jit(solution)/shard_map/all_to_all | solution.py:36
  128.8 8.9 %all-to-all-start.7 = ((bf16[4,8,256]{2,0,1:T(4,128)(2,1)}), bf16[4,8,256]{2,0,1:T(4,128)(2,1)S(1)}, u32[]{:S(2)}, u32[]{:S(2)}) async-start(bf16[4,8,256]{2,0,1:T(4,128)(2,1)} %bitcast.22), calls=%async_computation.7 | async-start | bytes 32768 | tf_op jit(solution)/shard_map/all_to_all | solution.py:184
  137.7 12.9 %all-to-all-start.5 = ((bf16[32,4,256]{2,1,0:T(4,128)(2,1)}), bf16[32,4,256]{2,1,0:T(4,128)(2,1)S(1)}, u32[]{:S(2)}, u32[]{:S(2)}) async-start(bf16[32,4,256]{2,1,0:T(4,128)(2,1)} %copy.86), calls=%async_computation.5 | async-start | bytes 131072 | tf_op jit(solution)/shard_map/all_to_all | solution.py:173
where the time goes:
time: 152 us; the launch traced here: 151 us
  starting transfers between devices  54.8 us (36%)
  waiting for transfers between devices  38.9 us (26%)
  blocking collectives  31.5 us (21%)
  matrix products  9.54 us (6%)
  local copies, waits for them, and re-layouts  8.99 us (6%)
  other arithmetic  6 us (4%)
  between operations  1.69 us (1%)
    all_gather x2, blocking collectives, gathered_by_axis(): array = lax.all_gather(array, axis, axis=dim, tiled=True)  31.5 us
    all_to_all x2, starting transfers between devices, sum_at_owner(): lax.all_to_all(split_up(array, dim, length), axis, 0, 0, tiled=True)  21.3 us
    all_to_all x2, waiting for transfers between devices, sum_at_owner(): lax.all_to_all(split_up(array, dim, length), axis, 0, 0, tiled=True)  17.1 us
    all_to_all x3, starting transfers between devices, sent_to_all(): return lax.all_to_all(copies, axis, split_axis=0, concat_axis=0, tiled=True)  14.6 us
    all_to_all x3, waiting for transfers between devices, sent_to_all(): return lax.all_to_all(copies, axis, split_axis=0, concat_axis=0, tiled=True)  12 us
    all_to_all x1, starting transfers between devices, per_device(): rows = lax.all_to_all(outgoing, EP, split_axis=0, concat_axis=0, tiled=True)  10.5 us
    all_to_all x1, waiting for transfers between devices, per_device(): lax.all_to_all(summed, EP, split_axis=0, concat_axis=0, tiled=True)  8.79 us
    all_to_all x1, starting transfers between devices, per_device(): lax.all_to_all(dense_own.astype(jnp.bfloat16), 'tp', split_axis=1, concat...  4.2 us
  transfers between devices with their start and end apart: 8, of which 7 were waited for; matrix products, arithmetic and copies ran while one was open for 9% of the time, Pallas kernels for 0%

commit v1 on v0

v1 whole, which is shorter than its diff:
```python
import functools

import jax
import jax.numpy as jnp
from jax import lax
from jax.experimental import pallas as pl
from jax.experimental.pallas import tpu as pltpu
from jax.sharding import PartitionSpec as P

EPS = 1e-06
MESH = pl.DeviceIdType.MESH
F32, BF16, I32 = jnp.float32, jnp.bfloat16, jnp.int32

NX, NZ, NTP, NEP = 4, 8, 8, 32
SEQ, D, WIDTH, DK, CAP = 32, 2048, 256, 128, 4
ROWS = NEP * CAP
FE, FD = 384, 128
PITCH = 72
CHUNKS = 4


def silu(v):
    return v * jax.nn.sigmoid(v)


def dot(a, b):
    return jnp.dot(a, b, preferred_element_type=F32)


def iota(shape, dim):
    return lax.broadcasted_iota(I32, shape, dim)


def kernel(
    hidden, state, attn_gain, wq, wk, wv, wg, w_beta, w_decay, decay_scale, head_gain, w_out, ffn_gain, ids, route,
    eg, eu, ed, dg, du, dd, mix,
    result, new_state,
    hid_all, v_state, v_again, v_wq, v_wk, v_wv, v_wg, v_wb, v_wd, v_dscale, v_hgain, v_wo, v_fgain, v_ids, v_route,
    v_eg, v_eu, v_ed, v_dg, v_du, v_dd, v_mix,
    xn_a, heads_all, mixed_s, send_mat, take_mat,
    disp, xa, stage, xn_e, inner_s, pb, pr, qs, yr, ret, rb,
    own_tok, dx, xn_d, px, xr, zs, zr, fs, fr,
    l_sem, out_sem,
    a_send, a_recv, h_send, h_recv, t_send, t_recv, d_send, d_recv, z_send, z_recv, x_send, x_recv,
    y_send, y_recv, c_send, c_recv, p_send, p_recv, q_send, q_recv, b_send, b_recv,
    u_send, u_recv, w_send, w_recv, f_send, f_recv,
):
    ep = lax.axis_index("ep")
    t = lax.axis_index("tp")
    z, x = lax.div(ep, NX), lax.rem(ep, NX)
    y, c = lax.div(t, 2), lax.rem(t, 2)

    def tp_peer(d):
        return ep, lax.rem(t + d, NTP)

    def ep_peer(d):
        return lax.rem(ep + d, NEP), t

    def z_peer(d):
        return lax.rem(z + d, NZ) * NX + x, t

    def x_peer(d):
        return z * NX + lax.rem(x + d, NX), t

    def y_peer(d):
        return ep, lax.rem(y + d, 4) * 2 + c

    partner = (ep, y * 2 + 1 - c)

    def remote(src, dst, send, recv, peer):
        return pltpu.make_async_remote_copy(
            src_ref=src, dst_ref=dst, send_sem=send, recv_sem=recv, device_id=peer, device_id_type=MESH
        )

    def take(view, sem):
        pltpu.make_async_copy(view, view, sem).wait()

    loads = {}
    pairs = (
        ("hid", hidden, hid_all.at[t]), ("ids", ids, v_ids), ("route", route, v_route), ("again", attn_gain, v_again),
        ("wq", wq, v_wq), ("wk", wk, v_wk), ("wv", wv, v_wv), ("wg", wg, v_wg), ("wb", w_beta, v_wb),
        ("wd", w_decay, v_wd), ("dscale", decay_scale, v_dscale), ("hgain", head_gain, v_hgain),
        ("state", state, v_state), ("wo", w_out, v_wo), ("fgain", ffn_gain, v_fgain), ("mix", mix, v_mix),
        ("dg", dg, v_dg), ("du", du, v_du), ("dd", dd, v_dd), ("eg", eg, v_eg), ("eu", eu, v_eu), ("ed", ed, v_ed),
    )
    for number, (name, src, dst) in enumerate(pairs):
        loads[name] = pltpu.make_async_copy(src, dst, l_sem.at[number])
        loads[name].start()

    barrier = pltpu.get_barrier_semaphore()
    for d in range(1, NTP):
        pl.semaphore_signal(barrier, inc=1, device_id=tp_peer(d), device_id_type=MESH)

    def greet(d, carry):
        pl.semaphore_signal(barrier, inc=1, device_id=ep_peer(d), device_id_type=MESH)
        return carry

    lax.fori_loop(1, NEP, greet, 0)

    loads["ids"].wait()
    loads["route"].wait()
    first, second = v_ids[:, 0:1], v_ids[:, 1:2]
    lane = iota((SEQ, NEP), 1)
    chosen = jnp.where((first == lane) | (second == lane), 1.0, 0.0)
    earlier = jnp.where(iota((SEQ, SEQ), 0) > iota((SEQ, SEQ), 1), 1.0, 0.0).astype(BF16)
    before = dot(earlier, chosen.astype(BF16))
    place = (chosen * (before + 1.0)).astype(BF16)
    row = iota((NEP * 8, NEP), 0)
    spread = jnp.where(row // 8 == iota((NEP * 8, NEP), 1), 1.0, 0.0).astype(BF16)
    by_row = lax.dot_general(spread, place, (((1,), (1,)), ((), ())), preferred_element_type=F32)
    want = ((row % 8) // 2 + 1).astype(F32)
    hit = by_row == want
    for h in range(2):
        send_mat[h] = jnp.where(hit & (row % 2 == h), 1.0, 0.0).astype(BF16)
    col = iota((SEQ, NEP * 8), 1)
    col_row = iota((NEP, NEP * 8), 1)
    spread_t = jnp.where(col_row // 8 == iota((NEP, NEP * 8), 0), 1.0, 0.0).astype(BF16)
    by_col = dot(place, spread_t)
    hit_t = by_col == ((col % 8) // 2 + 1).astype(F32)
    weight = jnp.where(first == col // 8, v_route[:, 0:1], 0.0) + jnp.where(second == col // 8, v_route[:, 1:2], 0.0)
    weight = jnp.where(hit_t, weight, 0.0)
    for h in range(2):
        part = jnp.where(col % 2 == h, weight, 0.0)
        high = part.astype(BF16)
        take_mat[2 * h] = high
        take_mat[2 * h + 1] = (part - high.astype(F32)).astype(BF16)

    loads["hid"].wait()
    pl.semaphore_wait(barrier, NTP - 1 + NEP - 1)

    copies = []
    for d in (4, 3, 5, 2, 6, 1, 7):
        copy = remote(hid_all.at[t], hid_all.at[t], a_send.at[d - 1], a_recv, tp_peer(d))
        copy.start()
        copies.append(copy)
    sends = copies
    loads["again"].wait()
    take(hid_all.at[pl.ds(0, 7)], a_recv)

    square = jnp.zeros((SEQ, WIDTH), F32)
    for b in range(NTP):
        wide = hid_all[b].astype(F32)
        square = square + wide * wide
    scale = lax.rsqrt(jnp.sum(square, axis=-1, keepdims=True) * (1.0 / D) + EPS)
    for b in range(NTP):
        cols = slice(b * WIDTH, (b + 1) * WIDTH)
        xn_a[:, cols] = (hid_all[b].astype(F32) * scale * v_again[:, cols]).astype(BF16)
    for name in ("wq", "wk", "wv", "wg", "wb", "wd", "dscale", "hgain"):
        loads[name].wait()
    normed = xn_a[...]
    queries = dot(normed, v_wq[...])
    queries = queries * lax.rsqrt(jnp.sum(queries * queries, axis=-1, keepdims=True) + EPS) * DK ** (-0.5)
    keys = dot(normed, v_wk[...])
    keys = keys * lax.rsqrt(jnp.sum(keys * keys, axis=-1, keepdims=True) + EPS)
    values = dot(normed, v_wv[...])
    gates = dot(normed, v_wg[...])
    mine = iota((SEQ, NTP), 1) == t
    beta = jax.nn.sigmoid(jnp.sum(jnp.where(mine, dot(normed, v_wb[...]), 0.0), axis=-1, keepdims=True))
    logit = jnp.sum(jnp.where(mine, dot(normed, v_wd[...]), 0.0), axis=-1, keepdims=True)
    d_scale = jnp.sum(jnp.where(iota((1, NTP), 1) == t, v_dscale[...], 0.0), axis=-1, keepdims=True)
    soft = jnp.maximum(logit, 0.0) + jnp.log(1.0 + jnp.exp(-jnp.abs(logit)))
    decay = jnp.exp(-d_scale * soft)

    loads["state"].wait()
    qb, kb = queries.astype(BF16), keys.astype(BF16)
    diag = iota((16, 1024), 1) // DK == iota((16, 1024), 0) % 8
    by_query, by_key = [], []
    for i in range(SEQ // 8):
        both = jnp.concatenate([qb[8 * i : 8 * i + 8].astype(F32), kb[8 * i : 8 * i + 8].astype(F32)], axis=0)
        lhs = jnp.where(diag, jnp.concatenate([both] * 8, axis=1), 0.0).astype(BF16)
        rhs = v_state[8 * i : 8 * i + 8].reshape(1024, DK).astype(BF16)
        out = dot(lhs, rhs)
        by_query.append(out[:8])
        by_key.append(out[8:])
    s_q = jnp.concatenate(by_query, axis=0)
    s_k = jnp.concatenate(by_key, axis=0)
    match = beta * jnp.sum(queries * keys, axis=-1, keepdims=True)
    read = decay * (s_q - match * s_k) + match * values
    read = read * lax.rsqrt(jnp.mean(read * read, axis=-1, keepdims=True) + EPS) * v_hgain[...]
    heads_all[t] = (read * silu(gates)).astype(BF16)
    for d in (4, 3, 5, 2, 6, 1, 7):
        copy = remote(heads_all.at[t], heads_all.at[t], h_send.at[d - 1], h_recv, tp_peer(d))
        copy.start()
        sends.append(copy)

    update = beta * (values - decay * s_k)
    keys_t = jnp.concatenate([keys, jnp.zeros((DK - SEQ, DK), F32)], axis=0).T
    decay_rows = jnp.broadcast_to(decay, (SEQ, DK))
    for s in range(SEQ):
        v_state[s] = decay_rows[s : s + 1] * v_state[s] + keys_t[:, s : s + 1] * update[s : s + 1]
    state_out = pltpu.make_async_copy(v_state, new_state, out_sem)
    state_out.start()

    loads["wo"].wait()
    take(heads_all.at[pl.ds(0, 7)], h_recv)
    wide = hid_all[t].astype(F32)
    for b in range(NTP):
        wide = wide + dot(heads_all[b], v_wo[b * DK : (b + 1) * DK, :])
    mixed = wide.astype(BF16)
    mixed_s[...] = mixed
    low, high = mixed[:, :128], mixed[:, 128:]

    t_row, t_col = iota((NTP * 8, SEQ), 0), iota((NTP * 8, SEQ), 1)
    pick = t_row // 2 == t_col
    pick_low = jnp.where(pick & (t_row % 2 == 0), 1.0, 0.0).astype(BF16)
    pick_high = jnp.where(pick & (t_row % 2 == 1), 1.0, 0.0).astype(BF16)
    tokens = (dot(pick_low, low) + dot(pick_high, high)).reshape(NTP, 8, 128).astype(BF16)
    own_tok[...] = tokens
    for d in (4, 3, 5, 2, 6, 1, 7):
        to = lax.rem(t + d, NTP)
        copy = remote(own_tok.at[to], dx.at[ep, t], t_send.at[d - 1], t_recv, tp_peer(d))
        copy.start()
        sends.append(copy)
    dx[ep, t] = own_tok[t]

    routed = dot(send_mat[0], low) + dot(send_mat[1], high)
    disp[...] = routed.reshape(NEP, 8, 128).astype(BF16)

    def dispatch(d, carry):
        to = lax.rem(ep + d, NEP)
        remote(disp.at[to], xa.at[t, ep], d_send, d_recv, ep_peer(d)).start()
        return carry

    lax.fori_loop(1, NEP, dispatch, 0)
    xa[t, ep] = disp[ep]

    take(dx.at[0, pl.ds(0, 7)], t_recv)

    def over_x(dz):
        block = lax.rem(z + NZ - dz, NZ) * NX + x
        for d in (2, 1, 3):
            copy = remote(dx.at[block], dx.at[block], x_send.at[d - 1, dz], x_recv.at[d - 1, dz], x_peer(d))
            copy.start()
            sends.append(copy)

    z_copies = {}
    for d in (4, 3, 5, 2, 6, 1, 7):
        copy = remote(dx.at[ep], dx.at[ep], z_send.at[d - 1], z_recv.at[d - 1], z_peer(d))
        copy.start()
        sends.append(copy)
        z_copies[d] = copy
    over_x(0)
    for d in (1, 7, 2, 6):
        z_copies[d].wait_recv()
        over_x(d)

    take(xa.at[0, pl.ds(0, NEP - 1)], d_recv)
    y_copies = {}
    for d in (2, 1, 3):
        copy = remote(xa.at[t], xa.at[t], y_send.at[d - 1], y_recv.at[d - 1], y_peer(d))
        copy.start()
        sends.append(copy)
        y_copies[d] = copy

    c_copies = []

    def across(d):
        slot = lax.rem(y + 4 - d, 4) * 2 + c
        copy = remote(xa.at[slot], xa.at[slot], c_send.at[d], c_recv.at[d], partner)
        copy.start()
        sends.append(copy)
        c_copies.append(copy)

    across(0)
    for d in (3, 5, 4):
        z_copies[d].wait_recv()
        over_x(d)
    for d in (1, 3, 2):
        y_copies[d].wait_recv()
        across(d)

    loads["fgain"].wait()
    for name in ("dg", "du", "dd"):
        loads[name].wait()
    for d in range(1, NX):
        for dz in range(NZ):
            remote(dx.at[0], dx.at[0], x_send.at[d - 1, dz], x_recv.at[d - 1, dz], x_peer(d)).wait_recv()
    for xx in range(NX):
        for zz in range(NZ):
            stage[pl.ds(zz * PITCH, 64), :] = dx[zz * NX + xx].astype(F32).reshape(64, 128)
        square = [jnp.zeros((8, 128), F32) for _ in range(4)]
        for j in range(4):
            for b in range(16):
                part = stage[pl.ds((b // 2) * 8 + j * 2 + b % 2, 8, stride=PITCH), :]
                square[j] = square[j] + part * part
        scales = [lax.rsqrt(jnp.sum(sq, axis=-1, keepdims=True) * (1.0 / D) + EPS) for sq in square]
        for b in range(16):
            cols = slice(b * 128, (b + 1) * 128)
            parts = [
                stage[pl.ds((b // 2) * 8 + j * 2 + b % 2, 8, stride=PITCH), :] * scales[j] * v_fgain[:, cols]
                for j in range(4)
            ]
            xn_d[xx * 32 : (xx + 1) * 32, cols] = jnp.concatenate(parts, axis=0).astype(BF16)
    rows_d = xn_d[...]
    hidden_d = (silu(dot(rows_d, v_dg[...])) * dot(rows_d, v_du[...])).astype(BF16)
    wide_f = D // CHUNKS
    for f in range(CHUNKS):
        out = dot(hidden_d, v_dd[:, f * wide_f : (f + 1) * wide_f]).astype(BF16)
        for xx in range(NX):
            px[xx, f] = out[xx * 32 : (xx + 1) * 32]
    u_copies = {}
    for f in range(CHUNKS):
        for d in (2, 1, 3):
            copy = remote(
                px.at[lax.rem(x + d, NX), f], xr.at[d - 1, f], u_send.at[d - 1, f], u_recv.at[d - 1, f], x_peer(d)
            )
            copy.start()
            sends.append(copy)
            u_copies[d, f] = copy

    for name in ("eg", "eu", "ed"):
        loads[name].wait()
    for copy in c_copies:
        copy.wait_recv()
    square = jnp.zeros((ROWS, 128), F32)
    for b in range(NTP):
        stage[pl.ds(0, 256), :] = xa[b].astype(F32).reshape(256, 128)
        for h in range(2):
            part = stage[pl.ds(h, ROWS, stride=2), :]
            square = square + part * part
            xn_e[:, b * WIDTH + h * 128 : b * WIDTH + (h + 1) * 128] = part.astype(BF16)
    scale = lax.rsqrt(jnp.sum(square, axis=-1, keepdims=True) * (1.0 / D) + EPS)
    for b in range(NTP):
        cols = slice(b * WIDTH, (b + 1) * WIDTH)
        xn_e[:, cols] = (xn_e[:, cols].astype(F32) * scale * v_fgain[:, cols]).astype(BF16)
    rows_e = xn_e[...]
    inner_s[...] = (silu(dot(rows_e, v_eg[...])) * dot(rows_e, v_eu[...])).astype(BF16)
    inner = inner_s[...]
    for b in range(NTP):
        pb[b] = dot(inner, v_ed[:, b * WIDTH : (b + 1) * WIDTH]).astype(BF16)
    p_copies = {}
    for d in (2, 1, 3, 0):
        there = lax.rem(y + d, 4)
        copy = remote(pb.at[there * 2 + 1 - c], pr.at[there], p_send.at[d], p_recv.at[d], partner)
        copy.start()
        sends.append(copy)
        p_copies[d] = copy
    q_copies = {}
    for d in (2, 1, 3, 0):
        there = lax.rem(y + d, 4)
        p_copies[d].wait_recv()
        qs[there] = (pb[there * 2 + c].astype(F32) + pr[there].astype(F32)).astype(BF16)
        if d > 0:
            copy = remote(qs.at[there], yr.at[d - 1], q_send.at[d - 1], q_recv.at[d - 1], y_peer(d))
            copy.start()
            sends.append(copy)
            q_copies[d] = copy

    def sum_x(f):
        for d in (1, 3, 2):
            u_copies[d, f].wait_recv()
        total = px[x, f].astype(F32)
        for d in range(3):
            total = total + xr[d, f].astype(F32)
        for tt in range(2):
            for h in range(2):
                cols = slice(tt * WIDTH + h * 128, tt * WIDTH + (h + 1) * 128)
                for j in range(4):
                    stage[pl.ds(tt * 8 + j * 2 + h, 8, stride=PITCH), :] = total[j * 8 : (j + 1) * 8, cols]
        for zz in range(NZ):
            zs[zz, 2 * f : 2 * f + 2] = stage[pl.ds(zz * PITCH, 16), :].reshape(2, 8, 128).astype(BF16)
        for d in (4, 3, 5, 2, 6, 1, 7):
            to = lax.rem(z + d, NZ)
            copy = remote(
                zs.at[to, pl.ds(2 * f, 2)], zr.at[d - 1, pl.ds(2 * f, 2)], w_send.at[d - 1, f], w_recv.at[f], z_peer(d)
            )
            copy.start()
            sends.append(copy)

    for f in range(CHUNKS):
        sum_x(f)

    for d in (1, 3, 2):
        q_copies[d].wait_recv()
    total = qs[y].astype(F32)
    for d in range(3):
        total = total + yr[d].astype(F32)
    total = total.astype(BF16).astype(F32)
    for h in range(2):
        stage[pl.ds(h, ROWS, stride=2), :] = total[:, h * 128 : (h + 1) * 128]
    ret[...] = stage[pl.ds(0, 256), :].reshape(NEP, 8, 128).astype(BF16)

    def give_back(d, carry):
        to = lax.rem(ep + d, NEP)
        remote(ret.at[to], rb.at[ep], b_send, b_recv, ep_peer(d)).start()
        return carry

    lax.fori_loop(1, NEP, give_back, 0)
    rb[ep] = ret[ep]

    for f in range(CHUNKS):
        take(zr.at[:, pl.ds(2 * f, 2)], w_recv.at[f])
    total = zs[z].astype(F32)
    for d in range(NZ - 1):
        total = total + zr[d].astype(F32)
    fs[...] = total.astype(BF16)
    for d in (4, 3, 5, 2, 6, 1, 7):
        to = lax.rem(t + d, NTP)
        copy = remote(fs.at[to], fr.at[t], f_send.at[d - 1], f_recv, tp_peer(d))
        copy.start()
        sends.append(copy)
    fr[t] = fs[t]

    loads["mix"].wait()
    take(rb.at[pl.ds(0, NEP - 1)], b_recv)
    back = rb[...].astype(F32).reshape(NEP * 8, 128).astype(BF16)
    moe = []
    for h in range(2):
        moe.append(dot(take_mat[2 * h], back) + dot(take_mat[2 * h + 1], back))
    take(fr.at[pl.ds(0, 7)], f_recv)
    stage[pl.ds(0, 64), :] = fr[...].astype(F32).reshape(64, 128)
    for h in range(2):
        cols = slice(h * 128, (h + 1) * 128)
        dense = stage[pl.ds(h, SEQ, stride=2), :]
        result[:, cols] = (
            mixed_s[:, cols].astype(F32) + moe[h] + jax.nn.sigmoid(v_mix[:, cols]) * dense
        ).astype(BF16)

    for copy in sends:
        copy.wait_send()
    take(disp.at[pl.ds(0, NEP - 1)], d_send)
    take(ret.at[pl.ds(0, NEP - 1)], b_send)
    state_out.wait()


def per_device(
    hidden_in, state_in, attn_gain, w_query, w_key, w_value, w_gate, w_beta, w_decay, decay_scale, head_gain, w_output,
    ffn_gain, expert_ids, route_weight, expert_gate, expert_up, expert_down, dense_gate, dense_up, dense_down, dense_mix,
):
    operands = (
        hidden_in, state_in.reshape(SEQ, DK, DK), attn_gain.reshape(1, D), w_query, w_key, w_value, w_gate, w_beta,
        w_decay, decay_scale.reshape(1, NTP), head_gain.reshape(1, DK), w_output, ffn_gain.reshape(1, D), expert_ids,
        route_weight, expert_gate[0], expert_up[0], expert_down[0], dense_gate, dense_up, dense_down,
        dense_mix.reshape(1, WIDTH),
    )
    V = pltpu.VMEM
    vmem_of = [V((NTP, SEQ, WIDTH), BF16)] + [V(o.shape, o.dtype) for o in operands[1:]]
    dma = pltpu.SemaphoreType.DMA
    scratch = vmem_of + [
        V((SEQ, D), BF16), V((NTP, SEQ, DK), BF16), V((SEQ, WIDTH), BF16),
        V((2, NEP * 8, SEQ), BF16), V((4, SEQ, NEP * 8), BF16),
        V((NEP, 8, 128), BF16), V((NTP, NEP, 8, 128), BF16), V((NZ * PITCH, 128), F32), V((ROWS, D), BF16),
        V((ROWS, FE), BF16), V((NTP, ROWS, WIDTH), BF16), V((4, ROWS, WIDTH), BF16), V((4, ROWS, WIDTH), BF16),
        V((3, ROWS, WIDTH), BF16), V((NEP, 8, 128), BF16), V((NEP, 8, 128), BF16),
        V((NTP, 8, 128), BF16), V((NEP, NTP, 8, 128), BF16), V((ROWS, D), BF16),
        V((NX, CHUNKS, 32, D // CHUNKS), BF16), V((3, CHUNKS, 32, D // CHUNKS), BF16),
        V((NZ, NTP, 8, 128), BF16), V((NZ - 1, NTP, 8, 128), BF16), V((NTP, 8, 128), BF16), V((NTP, 8, 128), BF16),
        dma((22,)), dma,
        dma((7,)), dma, dma((7,)), dma, dma((7,)), dma, dma, dma, dma((7,)), dma((7,)), dma((3, 8)), dma((3, 8)),
        dma((3,)), dma((3,)), dma((4,)), dma((4,)), dma((4,)), dma((4,)), dma((3,)), dma((3,)), dma, dma,
        dma((3, CHUNKS)), dma((3, CHUNKS)), dma((7, CHUNKS)), dma((CHUNKS,)), dma((7,)), dma,
    ]
    result, new_state = pl.pallas_call(
        kernel,
        out_shape=(
            jax.ShapeDtypeStruct((SEQ, WIDTH), BF16),
            jax.ShapeDtypeStruct((SEQ, DK, DK), F32),
        ),
        in_specs=[pl.BlockSpec(memory_space=pl.ANY)] * len(operands),
        out_specs=(pl.BlockSpec(memory_space=pltpu.VMEM), pl.BlockSpec(memory_space=pl.ANY)),
        scratch_shapes=scratch,
        compiler_params=pltpu.CompilerParams(
            collective_id=0, has_side_effects=True, vmem_limit_bytes=56 * 1024 * 1024
        ),
    )(*operands)
    return result, new_state.reshape(state_in.shape)


def solution(mesh):
    return jax.shard_map(
        per_device,
        mesh=mesh,
        in_specs=(
            P("ep", "tp"), P("ep", "tp", None, None), P(), P(None, "tp"), P(None, "tp"), P(None, "tp"), P(None, "tp"),
            P(), P(), P(), P(), P(None, "tp"), P(), P("ep", None), P("ep", None), P("ep", None, "tp"),
            P("ep", None, "tp"), P("ep", "tp", None), P(None, "ep"), P(None, "ep"), P("ep", None), P("tp"),
        ),
        out_specs=(P("ep", "tp"), P("ep", "tp", None, None)),
        check_vma=False,
    )
```

time: 152 us -> 65.8 us (0.43)
  starting transfers between devices: 54.8 us -> 0 us
  Pallas kernels: 0 us -> 54.1 us
  waiting for transfers between devices: 38.9 us -> 0 us
  blocking collectives: 31.5 us -> 0 us
  matrix products: 9.54 us -> 0 us
  other arithmetic: 6 us -> 0 us
  local copies, waits for them, and re-layouts: 8.99 us -> 10.7 us
    all_to_all x8 -> x0, starting transfers between devices: 54.8 us -> none  [the longest x2 21.3 us: sum_at_owner(): lax.all_to_all(split_up(array, dim, length), axis, 0, 0, tiled=True)]
    pallas_call x0 -> x1, Pallas kernels: none -> 54.1 us  [per_device(): pl.pallas_call(kernel, out_shape=(jax.ShapeDtypeStruct((SEQ, WIDTH), BF16...]
    all_to_all x8 -> x0, waiting for transfers between devices: 38.9 us -> none  [the longest x2 17.1 us: sum_at_owner(): lax.all_to_all(split_up(array, dim, length), axis, 0, 0, tiled=True)]
    all_gather x2 -> x0, blocking collectives: 31.5 us -> none  [gathered_by_axis(): array = lax.all_gather(array, axis, axis=dim, tiled=True)]
    unnamed x35 -> x6, local copies, waits for them, and re-layouts: 0.89 us -> 10.7 us
    dot_general x16 -> x0, matrix products: 9.54 us -> none  [the longest x1 1.96 us: per_device(): gate_val = jnp.dot(flat, expert_gate[0], preferred_element_type=jnp.float32)]
    reshape x7 -> x0, local copies, waits for them, and re-layouts: 3.16 us -> none  [the longest x2 1.84 us: split_up(): return jnp.moveaxis(array.reshape(*before, length, -1, *after), dim, 0)]
    add x2 -> x0, other arithmetic: 2.94 us -> none  [the longest x1 2.94 us: delta_update(): return decay_rate[..., None, None] * erased + written]
  transfers between devices with their start and end apart: 8 -> 0, of which waited for: 7 -> 0; matrix products, arithmetic and copies ran while one was open for 9% -> 0% of each run, Pallas kernels for 0% -> 0%
where the time goes in v1:
time: 65.8 us; the launch traced here: 65.5 us
  Pallas kernels  54.1 us (82%)
  local copies, waits for them, and re-layouts  10.7 us (16%)
    pallas_call x1, Pallas kernels, per_device(): pl.pallas_call(kernel, out_shape=(jax.ShapeDtypeStruct((SEQ, WIDTH), BF16...  54.1 us
    unnamed x6, local copies, waits for them, and re-layouts  10.7 us

profile of v1, /device:TPU:1, one launch (start us, length us, event | category | flops | bytes accessed | tf_op | source)
XLA Modules:
  0.0 65.5 jit_solution(5306201070878492774)
XLA Ops:
  0.6 1.4 %copy.26.ids = s32[32,2]{1,0:T(8,128)} copy(s32[32,2]{0,1:T(2,128)} %param.35) | data formatting | bytes 512 | tf_op args[13]
  2.0 1.4 %copy.27.route = f32[32,2]{1,0:T(8,128)} copy(f32[32,2]{0,1:T(2,128)} %param.36) | data formatting | bytes 512 | tf_op args[14]
  3.3 1.8 %copy.24.w_beta = bf16[2048,8]{1,0:T(8,128)(2,1)} copy(bf16[2048,8]{0,1:T(8,128)(2,1)} %param.29) | data formatting | bytes 65536 | tf_op args[7]
  5.1 1.8 %copy.25.w_decay = bf16[2048,8]{1,0:T(8,128)(2,1)} copy(bf16[2048,8]{0,1:T(8,128)(2,1)} %param.30) | data formatting | bytes 65536 | tf_op args[8]
  6.9 54.1 %shard_map.221 = (bf16[32,256]{1,0:T(8,128)(2,1)}, f32[32,128,128]{2,1,0:T(8,128)}) custom-call(bf16[32,256]{1,0:T(8,128)(2,1)} %hidden.1, f32[32,128,128]{2,1,0:T(8,128)} %bitcast.12, f32[1,2048]{1,0:T(1,128)} %bitcast.17, bf16[2048,128]{1,0:T(8,128)(2,1)} %wq.1, bf16[2048,128]{1,0:T(8,128)(2,1)} %wk.1, bf16[2048,128]{1,0:T(8,128)(2,1)} %wv.1, ...), custom_call_target="tpu_custom_call" | custom-call | tf_op jit(solution)/shard_map/pallas_call | solution.py:453
  61.0 1.3 %copy.31 = bf16[32,256]{1,0:T(8,128)(2,1)} copy(bf16[32,256]{1,0:T(8,128)(2,1)} %get-tuple-element.10) | data formatting | bytes 32768
  62.3 3.1 %copy.32 = f32[32,1,128,128]{3,2,1,0:T(8,128)} copy(f32[32,1,128,128]{3,2,1,0:T(8,128)} %bitcast.13) | data formatting | bytes 4194304

commit v2 on v1

--- a/solution.py
+++ b/solution.py
@@ -25,6 +25,14 @@
 
 def dot(a, b):
     return jnp.dot(a, b, preferred_element_type=F32)
+
+
+def dot_t(a, b):
+    return lax.dot_general(a, b, (((1,), (1,)), ((), ())), preferred_element_type=F32)
+
+
+def t_dot(a, b):
+    return lax.dot_general(a, b, (((0,), (0,)), ((), ())), preferred_element_type=F32)
 
 
 def iota(shape, dim):
@@ -40,10 +48,10 @@
     xn_a, heads_all, mixed_s, send_mat, take_mat,
     disp, xa, stage, xn_e, inner_s, pb, pr, qs, yr, ret, rb,
     own_tok, dx, xn_d, px, xr, zs, zr, fs, fr,
-    l_sem, out_sem,
+    l_sem,
     a_send, a_recv, h_send, h_recv, t_send, t_recv, d_send, d_recv, z_send, z_recv, x_send, x_recv,
     y_send, y_recv, c_send, c_recv, p_send, p_recv, q_send, q_recv, b_send, b_recv,
-    u_send, u_recv, w_send, w_recv, f_send, f_recv,
+    u_send, u_recv, w_send, w_recv, f_send, f_recv, met,
 ):
     ep = lax.axis_index("ep")
     t = lax.axis_index("tp")
@@ -88,45 +96,38 @@
         loads[name].start()
 
     barrier = pltpu.get_barrier_semaphore()
-    for d in range(1, NTP):
-        pl.semaphore_signal(barrier, inc=1, device_id=tp_peer(d), device_id_type=MESH)
-
-    def greet(d, carry):
-        pl.semaphore_signal(barrier, inc=1, device_id=ep_peer(d), device_id_type=MESH)
-        return carry
-
-    lax.fori_loop(1, NEP, greet, 0)
+    near = [tp_peer(d) for d in range(1, NTP)] + [z_peer(1), z_peer(NZ - 1), x_peer(1), x_peer(NX - 1)]
+    for peer in near:
+        pl.semaphore_signal(barrier, inc=1, device_id=peer, device_id_type=MESH)
+
+    def tell(number, peers):
+        for peer in peers:
+            pl.semaphore_signal(met.at[number], inc=1, device_id=peer, device_id_type=MESH)
 
     loads["ids"].wait()
     loads["route"].wait()
-    first, second = v_ids[:, 0:1], v_ids[:, 1:2]
-    lane = iota((SEQ, NEP), 1)
-    chosen = jnp.where((first == lane) | (second == lane), 1.0, 0.0)
-    earlier = jnp.where(iota((SEQ, SEQ), 0) > iota((SEQ, SEQ), 1), 1.0, 0.0).astype(BF16)
-    before = dot(earlier, chosen.astype(BF16))
+    first, second = v_ids[0:1, :], v_ids[1:2, :]
+    expert = iota((NEP, SEQ), 0)
+    is_first, is_second = first == expert, second == expert
+    chosen = jnp.where(is_first | is_second, 1.0, 0.0)
+    earlier = jnp.where(iota((SEQ, SEQ), 0) < iota((SEQ, SEQ), 1), 1.0, 0.0).astype(BF16)
+    before = dot(chosen.astype(BF16), earlier)
     place = (chosen * (before + 1.0)).astype(BF16)
     row = iota((NEP * 8, NEP), 0)
     spread = jnp.where(row // 8 == iota((NEP * 8, NEP), 1), 1.0, 0.0).astype(BF16)
-    by_row = lax.dot_general(spread, place, (((1,), (1,)), ((), ())), preferred_element_type=F32)
-    want = ((row % 8) // 2 + 1).astype(F32)
-    hit = by_row == want
+    hit = dot(spread, place) == ((row % 8) // 2 + 1).astype(F32)
+    weight = jnp.where(is_first, v_route[0:1, :], 0.0) + jnp.where(is_second, v_route[1:2, :], 0.0)
+    coarse = weight.astype(BF16)
+    fine = (weight - coarse.astype(F32)).astype(BF16)
+    coarse, fine = dot(spread, coarse), dot(spread, fine)
     for h in range(2):
-        send_mat[h] = jnp.where(hit & (row % 2 == h), 1.0, 0.0).astype(BF16)
-    col = iota((SEQ, NEP * 8), 1)
-    col_row = iota((NEP, NEP * 8), 1)
-    spread_t = jnp.where(col_row // 8 == iota((NEP, NEP * 8), 0), 1.0, 0.0).astype(BF16)
-    by_col = dot(place, spread_t)
-    hit_t = by_col == ((col % 8) // 2 + 1).astype(F32)
-    weight = jnp.where(first == col // 8, v_route[:, 0:1], 0.0) + jnp.where(second == col // 8, v_route[:, 1:2], 0.0)
-    weight = jnp.where(hit_t, weight, 0.0)
-    for h in range(2):
-        part = jnp.where(col % 2 == h, weight, 0.0)
-        high = part.astype(BF16)
-        take_mat[2 * h] = high
-        take_mat[2 * h + 1] = (part - high.astype(F32)).astype(BF16)
+        here = hit & (row % 2 == h)
+        send_mat[h] = jnp.where(here, 1.0, 0.0).astype(BF16)
+        take_mat[2 * h] = jnp.where(here, coarse, 0.0).astype(BF16)
+        take_mat[2 * h + 1] = jnp.where(here, fine, 0.0).astype(BF16)
 
     loads["hid"].wait()
-    pl.semaphore_wait(barrier, NTP - 1 + NEP - 1)
+    pl.semaphore_wait(barrier, len(near))
 
     copies = []
     for d in (4, 3, 5, 2, 6, 1, 7):
@@ -134,9 +135,12 @@
         copy.start()
         copies.append(copy)
     sends = copies
+    tell(0, (z_peer(1), z_peer(NZ - 1), x_peer(1), x_peer(NX - 1)))
     loads["again"].wait()
     take(hid_all.at[pl.ds(0, 7)], a_recv)
 
+    pl.semaphore_wait(met.at[0], 4)
+    tell(1, (z_peer(2), z_peer(NZ - 2)))
     square = jnp.zeros((SEQ, WIDTH), F32)
     for b in range(NTP):
         wide = hid_all[b].astype(F32)
@@ -155,8 +159,8 @@
     values = dot(normed, v_wv[...])
     gates = dot(normed, v_wg[...])
     mine = iota((SEQ, NTP), 1) == t
-    beta = jax.nn.sigmoid(jnp.sum(jnp.where(mine, dot(normed, v_wb[...]), 0.0), axis=-1, keepdims=True))
-    logit = jnp.sum(jnp.where(mine, dot(normed, v_wd[...]), 0.0), axis=-1, keepdims=True)
+    beta = jax.nn.sigmoid(jnp.sum(jnp.where(mine, dot_t(normed, v_wb[...]), 0.0), axis=-1, keepdims=True))
+    logit = jnp.sum(jnp.where(mine, dot_t(normed, v_wd[...]), 0.0), axis=-1, keepdims=True)
     d_scale = jnp.sum(jnp.where(iota((1, NTP), 1) == t, v_dscale[...], 0.0), axis=-1, keepdims=True)
     soft = jnp.maximum(logit, 0.0) + jnp.log(1.0 + jnp.exp(-jnp.abs(logit)))
     decay = jnp.exp(-d_scale * soft)
@@ -183,14 +187,15 @@
         copy.start()
         sends.append(copy)
 
+    pl.semaphore_wait(met.at[1], 2)
+    tell(2, (x_peer(1), x_peer(2), x_peer(3)))
     update = beta * (values - decay * s_k)
     keys_t = jnp.concatenate([keys, jnp.zeros((DK - SEQ, DK), F32)], axis=0).T
     decay_rows = jnp.broadcast_to(decay, (SEQ, DK))
     for s in range(SEQ):
-        v_state[s] = decay_rows[s : s + 1] * v_state[s] + keys_t[:, s : s + 1] * update[s : s + 1]
-    state_out = pltpu.make_async_copy(v_state, new_state, out_sem)
-    state_out.start()
-
+        new_state[s] = decay_rows[s : s + 1] * v_state[s] + keys_t[:, s : s + 1] * update[s : s + 1]
+
+    pl.semaphore_wait(met.at[2], 3)
     loads["wo"].wait()
     take(heads_all.at[pl.ds(0, 7)], h_recv)
     wide = hid_all[t].astype(F32)
@@ -406,7 +411,7 @@
     back = rb[...].astype(F32).reshape(NEP * 8, 128).astype(BF16)
     moe = []
     for h in range(2):
-        moe.append(dot(take_mat[2 * h], back) + dot(take_mat[2 * h + 1], back))
+        moe.append(t_dot(take_mat[2 * h], back) + t_dot(take_mat[2 * h + 1], back))
     take(fr.at[pl.ds(0, 7)], f_recv)
     stage[pl.ds(0, 64), :] = fr[...].astype(F32).reshape(64, 128)
     for h in range(2):
@@ -420,7 +425,15 @@
         copy.wait_send()
     take(disp.at[pl.ds(0, NEP - 1)], d_send)
     take(ret.at[pl.ds(0, NEP - 1)], b_send)
-    state_out.wait()
+
+
+def write_out(result, new_state, result_out, state_out, sem):
+    first = pltpu.make_async_copy(result, result_out, sem.at[0])
+    second = pltpu.make_async_copy(new_state, state_out, sem.at[1])
+    first.start()
+    second.start()
+    first.wait()
+    second.wait()
 
 
 def per_device(
@@ -428,9 +441,9 @@
     ffn_gain, expert_ids, route_weight, expert_gate, expert_up, expert_down, dense_gate, dense_up, dense_down, dense_mix,
 ):
     operands = (
-        hidden_in, state_in.reshape(SEQ, DK, DK), attn_gain.reshape(1, D), w_query, w_key, w_value, w_gate, w_beta,
-        w_decay, decay_scale.reshape(1, NTP), head_gain.reshape(1, DK), w_output, ffn_gain.reshape(1, D), expert_ids,
-        route_weight, expert_gate[0], expert_up[0], expert_down[0], dense_gate, dense_up, dense_down,
+        hidden_in, state_in.reshape(SEQ, DK, DK), attn_gain.reshape(1, D), w_query, w_key, w_value, w_gate, w_beta.T,
+        w_decay.T, decay_scale.reshape(1, NTP), head_gain.reshape(1, DK), w_output, ffn_gain.reshape(1, D), expert_ids.T,
+        route_weight.T, expert_gate[0], expert_up[0], expert_down[0], dense_gate, dense_up, dense_down,
         dense_mix.reshape(1, WIDTH),
     )
     V = pltpu.VMEM
@@ -438,31 +451,38 @@
     dma = pltpu.SemaphoreType.DMA
     scratch = vmem_of + [
         V((SEQ, D), BF16), V((NTP, SEQ, DK), BF16), V((SEQ, WIDTH), BF16),
-        V((2, NEP * 8, SEQ), BF16), V((4, SEQ, NEP * 8), BF16),
+        V((2, NEP * 8, SEQ), BF16), V((4, NEP * 8, SEQ), BF16),
         V((NEP, 8, 128), BF16), V((NTP, NEP, 8, 128), BF16), V((NZ * PITCH, 128), F32), V((ROWS, D), BF16),
         V((ROWS, FE), BF16), V((NTP, ROWS, WIDTH), BF16), V((4, ROWS, WIDTH), BF16), V((4, ROWS, WIDTH), BF16),
         V((3, ROWS, WIDTH), BF16), V((NEP, 8, 128), BF16), V((NEP, 8, 128), BF16),
         V((NTP, 8, 128), BF16), V((NEP, NTP, 8, 128), BF16), V((ROWS, D), BF16),
         V((NX, CHUNKS, 32, D // CHUNKS), BF16), V((3, CHUNKS, 32, D // CHUNKS), BF16),
         V((NZ, NTP, 8, 128), BF16), V((NZ - 1, NTP, 8, 128), BF16), V((NTP, 8, 128), BF16), V((NTP, 8, 128), BF16),
-        dma((22,)), dma,
+        dma((22,)),
         dma((7,)), dma, dma((7,)), dma, dma((7,)), dma, dma, dma, dma((7,)), dma((7,)), dma((3, 8)), dma((3, 8)),
         dma((3,)), dma((3,)), dma((4,)), dma((4,)), dma((4,)), dma((4,)), dma((3,)), dma((3,)), dma, dma,
         dma((3, CHUNKS)), dma((3, CHUNKS)), dma((7, CHUNKS)), dma((CHUNKS,)), dma((7,)), dma,
+        pltpu.SemaphoreType.REGULAR((3,)),
     ]
+    kept = (V((SEQ, WIDTH), BF16), V((SEQ, DK, DK), F32))
     result, new_state = pl.pallas_call(
         kernel,
-        out_shape=(
-            jax.ShapeDtypeStruct((SEQ, WIDTH), BF16),
-            jax.ShapeDtypeStruct((SEQ, DK, DK), F32),
-        ),
-        in_specs=[pl.BlockSpec(memory_space=pl.ANY)] * len(operands),
-        out_specs=(pl.BlockSpec(memory_space=pltpu.VMEM), pl.BlockSpec(memory_space=pl.ANY)),
+        out_shape=kept,
+        in_specs=[pl.BlockSpec(memory_space=pltpu.HBM)] * len(operands),
+        out_specs=tuple(pl.BlockSpec(memory_space=pltpu.VMEM) for _ in kept),
         scratch_shapes=scratch,
         compiler_params=pltpu.CompilerParams(
-            collective_id=0, has_side_effects=True, vmem_limit_bytes=56 * 1024 * 1024
+            collective_id=0, has_side_effects=True, vmem_limit_bytes=64000000
         ),
     )(*operands)
+    result, new_state = pl.pallas_call(
+        write_out,
+        out_shape=tuple(jax.ShapeDtypeStruct(k.shape, k.dtype) for k in kept),
+        in_specs=[pl.BlockSpec(memory_space=pltpu.VMEM)] * 2,
+        out_specs=tuple(pl.BlockSpec(memory_space=pltpu.HBM) for _ in kept),
+        scratch_shapes=[dma((2,))],
+        compiler_params=pltpu.CompilerParams(vmem_limit_bytes=8 * 1024 * 1024),
+    )(result, new_state)
     return result, new_state.reshape(state_in.shape)
 
 

time: 65.8 us -> 54.4 us (0.83)
  local copies, waits for them, and re-layouts: 10.7 us -> 0 us
    unnamed x6 -> x0, local copies, waits for them, and re-layouts: 10.7 us -> none
    pallas_call x1 -> x2, Pallas kernels: 54.1 us -> 53.7 us  [the longest x1 52.3 us: per_device(): pl.pallas_call(kernel, out_shape=kept, in_specs=[pl.BlockSpec(memory_spac...]
where the time goes in v2:
time: 54.4 us; the launch traced here: 54.3 us
  Pallas kernels  53.7 us (99%)
  between operations  0.65 us (1%)
    pallas_call x1, Pallas kernels, per_device(): pl.pallas_call(kernel, out_shape=kept, in_specs=[pl.BlockSpec(memory_spac...  52.3 us
    pallas_call x1, Pallas kernels, per_device(): pl.pallas_call(write_out, out_shape=tuple((jax.ShapeDtypeStruct(k.shape,...  1.34 us

profile of v2, /device:TPU:1, one launch (start us, length us, event | category | flops | bytes accessed | tf_op | source)
XLA Modules:
  0.0 54.3 jit_solution(8958954323728250544)
XLA Ops:
  0.6 52.3 %shard_map.221 = (bf16[32,256]{1,0:T(8,128)(2,1)S(1)}, f32[32,128,128]{2,1,0:T(8,128)S(1)}) custom-call(bf16[32,256]{1,0:T(8,128)(2,1)} %hidden.1, f32[32,128,128]{2,1,0:T(8,128)} %bitcast.16, f32[1,2048]{1,0:T(1,128)} %bitcast.22, bf16[2048,128]{1,0:T(8,128)(2,1)} %wq.1, bf16[2048,128]{1,0:T(8,128)(2,1)} %wk.1, bf16[2048,128]{1,0:T(8,128)(2,1)} %wv.1, ...), custom_call_target="tpu_custom_call" | custom-call | tf_op jit(solution)/shard_map/pallas_call | solution.py:468
  53.0 1.3 %shard_map.222 = (bf16[32,256]{1,0:T(8,128)(2,1)}, f32[32,128,128]{2,1,0:T(8,128)}) custom-call(bf16[32,256]{1,0:T(8,128)(2,1)S(1)} %get-tuple-element.6.result, f32[32,128,128]{2,1,0:T(8,128)S(1)} %get-tuple-element.7.new_state), custom_call_target="tpu_custom_call" | custom-call | tf_op jit(solution)/shard_map/pallas_call | solution.py:478

commit v3 on v2

--- a/solution.py
+++ b/solution.py
@@ -17,6 +17,8 @@
 FE, FD = 384, 128
 PITCH = 72
 CHUNKS = 4
+WIDE = D // CHUNKS
+FAR_TP = FAR_Z = (4, 3, 5, 2, 6, 1, 7)
 
 
 def silu(v):
@@ -47,11 +49,8 @@
     v_eg, v_eu, v_ed, v_dg, v_du, v_dd, v_mix,
     xn_a, heads_all, mixed_s, send_mat, take_mat,
     disp, xa, stage, xn_e, inner_s, pb, pr, qs, yr, ret, rb,
-    own_tok, dx, xn_d, px, xr, zs, zr, fs, fr,
-    l_sem,
-    a_send, a_recv, h_send, h_recv, t_send, t_recv, d_send, d_recv, z_send, z_recv, x_send, x_recv,
-    y_send, y_recv, c_send, c_recv, p_send, p_recv, q_send, q_recv, b_send, b_recv,
-    u_send, u_recv, w_send, w_recv, f_send, f_recv, met,
+    own_tok, dx, xn_d, px, xr, zs, fr,
+    l_sem, send, a_recv, h_recv, t_recv, d_recv, x_recv, y_recv, c_recv, p_recv, q_recv, b_recv, u_recv, w_recv, met,
 ):
     ep = lax.axis_index("ep")
     t = lax.axis_index("tp")
@@ -75,10 +74,10 @@
 
     partner = (ep, y * 2 + 1 - c)
 
-    def remote(src, dst, send, recv, peer):
-        return pltpu.make_async_remote_copy(
-            src_ref=src, dst_ref=dst, send_sem=send, recv_sem=recv, device_id=peer, device_id_type=MESH
-        )
+    def remote(src, dst, phase, recv, peer):
+        pltpu.make_async_remote_copy(
+            src_ref=src, dst_ref=dst, send_sem=send.at[phase], recv_sem=recv, device_id=peer, device_id_type=MESH
+        ).start()
 
     def take(view, sem):
         pltpu.make_async_copy(view, view, sem).wait()
@@ -129,12 +128,8 @@
     loads["hid"].wait()
     pl.semaphore_wait(barrier, len(near))
 
-    copies = []
-    for d in (4, 3, 5, 2, 6, 1, 7):
-        copy = remote(hid_all.at[t], hid_all.at[t], a_send.at[d - 1], a_recv, tp_peer(d))
-        copy.start()
-        copies.append(copy)
-    sends = copies
+    for d in FAR_TP:
+        remote(hid_all.at[t], hid_all.at[t], 0, a_recv, tp_peer(d))
     tell(0, (z_peer(1), z_peer(NZ - 1), x_peer(1), x_peer(NX - 1)))
     loads["again"].wait()
     take(hid_all.at[pl.ds(0, 7)], a_recv)
@@ -182,20 +177,17 @@
     read = decay * (s_q - match * s_k) + match * values
     read = read * lax.rsqrt(jnp.mean(read * read, axis=-1, keepdims=True) + EPS) * v_hgain[...]
     heads_all[t] = (read * silu(gates)).astype(BF16)
-    for d in (4, 3, 5, 2, 6, 1, 7):
-        copy = remote(heads_all.at[t], heads_all.at[t], h_send.at[d - 1], h_recv, tp_peer(d))
-        copy.start()
-        sends.append(copy)
-
+    for d in FAR_TP:
+        remote(heads_all.at[t], heads_all.at[t], 1, h_recv, tp_peer(d))
     pl.semaphore_wait(met.at[1], 2)
-    tell(2, (x_peer(1), x_peer(2), x_peer(3)))
+    tell(2, (x_peer(1), x_peer(2), x_peer(3), z_peer(NZ // 2)))
     update = beta * (values - decay * s_k)
     keys_t = jnp.concatenate([keys, jnp.zeros((DK - SEQ, DK), F32)], axis=0).T
     decay_rows = jnp.broadcast_to(decay, (SEQ, DK))
     for s in range(SEQ):
         new_state[s] = decay_rows[s : s + 1] * v_state[s] + keys_t[:, s : s + 1] * update[s : s + 1]
 
-    pl.semaphore_wait(met.at[2], 3)
+    pl.semaphore_wait(met.at[2], 4)
     loads["wo"].wait()
     take(heads_all.at[pl.ds(0, 7)], h_recv)
     wide = hid_all[t].astype(F32)
@@ -209,78 +201,51 @@
     pick = t_row // 2 == t_col
     pick_low = jnp.where(pick & (t_row % 2 == 0), 1.0, 0.0).astype(BF16)
     pick_high = jnp.where(pick & (t_row % 2 == 1), 1.0, 0.0).astype(BF16)
-    tokens = (dot(pick_low, low) + dot(pick_high, high)).reshape(NTP, 8, 128).astype(BF16)
-    own_tok[...] = tokens
-    for d in (4, 3, 5, 2, 6, 1, 7):
-        to = lax.rem(t + d, NTP)
-        copy = remote(own_tok.at[to], dx.at[ep, t], t_send.at[d - 1], t_recv, tp_peer(d))
-        copy.start()
-        sends.append(copy)
+    own_tok[...] = (dot(pick_low, low) + dot(pick_high, high)).reshape(NTP, 8, 128).astype(BF16)
+
+    def tokens(dz):
+        def body(d, carry):
+            to = lax.rem(t + d, NTP)
+            remote(own_tok.at[to], dx.at[ep, t], 2, t_recv.at[dz], (z_peer(dz)[0], to))
+            return carry
+
+        lax.fori_loop(1 if dz == 0 else 0, NTP, body, 0)
+
+    for dz in FAR_Z:
+        tokens(dz)
+    tokens(0)
     dx[ep, t] = own_tok[t]
-
-    routed = dot(send_mat[0], low) + dot(send_mat[1], high)
-    disp[...] = routed.reshape(NEP, 8, 128).astype(BF16)
-
-    def dispatch(d, carry):
-        to = lax.rem(ep + d, NEP)
-        remote(disp.at[to], xa.at[t, ep], d_send, d_recv, ep_peer(d)).start()
-        return carry
-
-    lax.fori_loop(1, NEP, dispatch, 0)
+    disp[...] = (dot(send_mat[0], low) + dot(send_mat[1], high)).reshape(NEP, 8, 128).astype(BF16)
+
+    def dispatch(dz):
+        def body(d, carry):
+            to = z_peer(dz)[0] - x + lax.rem(x + d, NX)
+            remote(disp.at[to], xa.at[t, ep], 3, d_recv.at[dz], (to, t))
+            return carry
+
+        lax.fori_loop(1 if dz == 0 else 0, NX, body, 0)
+
+    for dz in FAR_Z:
+        dispatch(dz)
+    dispatch(0)
     xa[t, ep] = disp[ep]
-
-    take(dx.at[0, pl.ds(0, 7)], t_recv)
-
-    def over_x(dz):
-        block = lax.rem(z + NZ - dz, NZ) * NX + x
+    for dz in (0, 1, 7, 2, 6, 3, 5, 4):
+        from_z = lax.rem(z + NZ - dz, NZ)
+        take(dx.at[0] if dz else dx.at[0, pl.ds(0, 7)], t_recv.at[dz])
+        block = dx.at[from_z * NX + x]
         for d in (2, 1, 3):
-            copy = remote(dx.at[block], dx.at[block], x_send.at[d - 1, dz], x_recv.at[d - 1, dz], x_peer(d))
-            copy.start()
-            sends.append(copy)
-
-    z_copies = {}
-    for d in (4, 3, 5, 2, 6, 1, 7):
-        copy = remote(dx.at[ep], dx.at[ep], z_send.at[d - 1], z_recv.at[d - 1], z_peer(d))
-        copy.start()
-        sends.append(copy)
-        z_copies[d] = copy
-    over_x(0)
-    for d in (1, 7, 2, 6):
-        z_copies[d].wait_recv()
-        over_x(d)
-
-    take(xa.at[0, pl.ds(0, NEP - 1)], d_recv)
-    y_copies = {}
-    for d in (2, 1, 3):
-        copy = remote(xa.at[t], xa.at[t], y_send.at[d - 1], y_recv.at[d - 1], y_peer(d))
-        copy.start()
-        sends.append(copy)
-        y_copies[d] = copy
-
-    c_copies = []
-
-    def across(d):
-        slot = lax.rem(y + 4 - d, 4) * 2 + c
-        copy = remote(xa.at[slot], xa.at[slot], c_send.at[d], c_recv.at[d], partner)
-        copy.start()
-        sends.append(copy)
-        c_copies.append(copy)
-
-    across(0)
-    for d in (3, 5, 4):
-        z_copies[d].wait_recv()
-        over_x(d)
-    for d in (1, 3, 2):
-        y_copies[d].wait_recv()
-        across(d)
-
+            remote(block, block, 4, x_recv.at[d - 1], x_peer(d))
+        take(disp.at[pl.ds(0, NX if dz else NX - 1)], d_recv.at[dz])
+        block = xa.at[t, pl.ds(from_z * NX, NX)]
+        for d in (2, 1, 3):
+            remote(block, block, 5, y_recv.at[d - 1], y_peer(d))
+        remote(block, block, 6, c_recv.at[0], partner)
     loads["fgain"].wait()
     for name in ("dg", "du", "dd"):
         loads[name].wait()
-    for d in range(1, NX):
-        for dz in range(NZ):
-            remote(dx.at[0], dx.at[0], x_send.at[d - 1, dz], x_recv.at[d - 1, dz], x_peer(d)).wait_recv()
-    for xx in range(NX):
+
+    def dense(d):
+        xx = lax.rem(x + NX - d, NX)
         for zz in range(NZ):
             stage[pl.ds(zz * PITCH, 64), :] = dx[zz * NX + xx].astype(F32).reshape(64, 128)
         square = [jnp.zeros((8, 128), F32) for _ in range(4)]
@@ -295,28 +260,27 @@
                 stage[pl.ds((b // 2) * 8 + j * 2 + b % 2, 8, stride=PITCH), :] * scales[j] * v_fgain[:, cols]
                 for j in range(4)
             ]
-            xn_d[xx * 32 : (xx + 1) * 32, cols] = jnp.concatenate(parts, axis=0).astype(BF16)
-    rows_d = xn_d[...]
-    hidden_d = (silu(dot(rows_d, v_dg[...])) * dot(rows_d, v_du[...])).astype(BF16)
-    wide_f = D // CHUNKS
-    for f in range(CHUNKS):
-        out = dot(hidden_d, v_dd[:, f * wide_f : (f + 1) * wide_f]).astype(BF16)
-        for xx in range(NX):
-            px[xx, f] = out[xx * 32 : (xx + 1) * 32]
-    u_copies = {}
-    for f in range(CHUNKS):
-        for d in (2, 1, 3):
-            copy = remote(
-                px.at[lax.rem(x + d, NX), f], xr.at[d - 1, f], u_send.at[d - 1, f], u_recv.at[d - 1, f], x_peer(d)
-            )
-            copy.start()
-            sends.append(copy)
-            u_copies[d, f] = copy
-
+            xn_d[d, :, cols] = jnp.concatenate(parts, axis=0).astype(BF16)
+        rows = xn_d[d]
+        hidden_d = (silu(dot(rows, v_dg[...])) * dot(rows, v_du[...])).astype(BF16)
+        for f in range(CHUNKS):
+            px[d, f] = dot(hidden_d, v_dd[:, f * WIDE : (f + 1) * WIDE]).astype(BF16)
+            if d:
+                back = NX - d
+                remote(px.at[d, f], xr.at[back - 1, f], 7, u_recv.at[back - 1, f], x_peer(back))
+
+    dense(0)
+    for d in (1, 3, 2):
+        take(xa.at[0], y_recv.at[d - 1])
+        block = xa.at[lax.rem(y + 4 - d, 4) * 2 + c]
+        remote(block, block, 6, c_recv.at[d], partner)
+    for d in (1, 3, 2):
+        take(dx.at[pl.ds(0, NZ)], x_recv.at[d - 1])
+        dense(d)
     for name in ("eg", "eu", "ed"):
         loads[name].wait()
-    for copy in c_copies:
-        copy.wait_recv()
+    for d in range(4):
+        take(xa.at[0], c_recv.at[d])
     square = jnp.zeros((ROWS, 128), F32)
     for b in range(NTP):
         stage[pl.ds(0, 256), :] = xa[b].astype(F32).reshape(256, 128)
@@ -333,28 +297,20 @@
     inner = inner_s[...]
     for b in range(NTP):
         pb[b] = dot(inner, v_ed[:, b * WIDTH : (b + 1) * WIDTH]).astype(BF16)
-    p_copies = {}
     for d in (2, 1, 3, 0):
         there = lax.rem(y + d, 4)
-        copy = remote(pb.at[there * 2 + 1 - c], pr.at[there], p_send.at[d], p_recv.at[d], partner)
-        copy.start()
-        sends.append(copy)
-        p_copies[d] = copy
-    q_copies = {}
+        remote(pb.at[there * 2 + 1 - c], pr.at[there], 8, p_recv.at[d], partner)
     for d in (2, 1, 3, 0):
         there = lax.rem(y + d, 4)
-        p_copies[d].wait_recv()
+        take(pr.at[0], p_recv.at[d])
         qs[there] = (pb[there * 2 + c].astype(F32) + pr[there].astype(F32)).astype(BF16)
         if d > 0:
-            copy = remote(qs.at[there], yr.at[d - 1], q_send.at[d - 1], q_recv.at[d - 1], y_peer(d))
-            copy.start()
-            sends.append(copy)
-            q_copies[d] = copy
+            remote(qs.at[there], yr.at[d - 1], 9, q_recv.at[d - 1], y_peer(d))
 
     def sum_x(f):
         for d in (1, 3, 2):
-            u_copies[d, f].wait_recv()
-        total = px[x, f].astype(F32)
+            take(xr.at[0, 0], u_recv.at[d - 1, f])
+        total = px[0, f].astype(F32)
         for d in range(3):
             total = total + xr[d, f].astype(F32)
         for tt in range(2):
@@ -364,19 +320,23 @@
                     stage[pl.ds(tt * 8 + j * 2 + h, 8, stride=PITCH), :] = total[j * 8 : (j + 1) * 8, cols]
         for zz in range(NZ):
             zs[zz, 2 * f : 2 * f + 2] = stage[pl.ds(zz * PITCH, 16), :].reshape(2, 8, 128).astype(BF16)
-        for d in (4, 3, 5, 2, 6, 1, 7):
-            to = lax.rem(z + d, NZ)
-            copy = remote(
-                zs.at[to, pl.ds(2 * f, 2)], zr.at[d - 1, pl.ds(2 * f, 2)], w_send.at[d - 1, f], w_recv.at[f], z_peer(d)
-            )
-            copy.start()
-            sends.append(copy)
+        for dz in FAR_Z + (0,):
+            to = z_peer(dz)[0]
+
+            def piece(tt):
+                remote(zs.at[lax.div(to, NX), tt], fr.at[z * NTP + t], 10, w_recv, (to, tt))
+
+            for tt in (2 * f, 2 * f + 1):
+                if dz:
+                    piece(tt)
+                else:
+                    pl.when(t != tt)(functools.partial(piece, tt))
 
     for f in range(CHUNKS):
         sum_x(f)
-
+    fr[z * NTP + t] = zs[z, t]
     for d in (1, 3, 2):
-        q_copies[d].wait_recv()
+        take(yr.at[0], q_recv.at[d - 1])
     total = qs[y].astype(F32)
     for d in range(3):
         total = total + yr[d].astype(F32)
@@ -386,45 +346,38 @@
     ret[...] = stage[pl.ds(0, 256), :].reshape(NEP, 8, 128).astype(BF16)
 
     def give_back(d, carry):
-        to = lax.rem(ep + d, NEP)
-        remote(ret.at[to], rb.at[ep], b_send, b_recv, ep_peer(d)).start()
+        to = lax.rem(ep + NEP // 2 + d, NEP)
+
+        @pl.when(to != ep)
+        def _():
+            remote(ret.at[to], rb.at[ep], 11, b_recv, (to, t))
+
         return carry
 
-    lax.fori_loop(1, NEP, give_back, 0)
+    lax.fori_loop(0, NEP, give_back, 0)
     rb[ep] = ret[ep]
-
-    for f in range(CHUNKS):
-        take(zr.at[:, pl.ds(2 * f, 2)], w_recv.at[f])
-    total = zs[z].astype(F32)
-    for d in range(NZ - 1):
-        total = total + zr[d].astype(F32)
-    fs[...] = total.astype(BF16)
-    for d in (4, 3, 5, 2, 6, 1, 7):
-        to = lax.rem(t + d, NTP)
-        copy = remote(fs.at[to], fr.at[t], f_send.at[d - 1], f_recv, tp_peer(d))
-        copy.start()
-        sends.append(copy)
-    fr[t] = fs[t]
-
     loads["mix"].wait()
+    take(fr.at[pl.ds(0, NZ * NTP - 1)], w_recv)
+    total = fr[0:NTP].astype(F32)
+    for zz in range(1, NZ):
+        total = total + fr[zz * NTP : (zz + 1) * NTP].astype(F32)
+    stage[pl.ds(0, 64), :] = total.reshape(64, 128)
     take(rb.at[pl.ds(0, NEP - 1)], b_recv)
     back = rb[...].astype(F32).reshape(NEP * 8, 128).astype(BF16)
-    moe = []
-    for h in range(2):
-        moe.append(t_dot(take_mat[2 * h], back) + t_dot(take_mat[2 * h + 1], back))
-    take(fr.at[pl.ds(0, 7)], f_recv)
-    stage[pl.ds(0, 64), :] = fr[...].astype(F32).reshape(64, 128)
     for h in range(2):
         cols = slice(h * 128, (h + 1) * 128)
-        dense = stage[pl.ds(h, SEQ, stride=2), :]
+        moe = t_dot(take_mat[2 * h], back) + t_dot(take_mat[2 * h + 1], back)
+        dense_out = stage[pl.ds(h, SEQ, stride=2), :]
         result[:, cols] = (
-            mixed_s[:, cols].astype(F32) + moe[h] + jax.nn.sigmoid(v_mix[:, cols]) * dense
+            mixed_s[:, cols].astype(F32) + moe + jax.nn.sigmoid(v_mix[:, cols]) * dense_out
         ).astype(BF16)
-
-    for copy in sends:
-        copy.wait_send()
-    take(disp.at[pl.ds(0, NEP - 1)], d_send)
-    take(ret.at[pl.ds(0, NEP - 1)], b_send)
+    sent = (
+        hid_all.at[pl.ds(0, 7)], heads_all.at[pl.ds(0, 7)], fr.at[pl.ds(0, 63)], disp.at[pl.ds(0, 31)],
+        dx.at[pl.ds(0, 24)], xa.at[pl.ds(0, 3)], xa.at[pl.ds(0, 4)], px.at[pl.ds(0, 3)], pb.at[pl.ds(0, 4)],
+        qs.at[pl.ds(0, 3)], fr.at[pl.ds(0, 63)], ret.at[pl.ds(0, 31)],
+    )
+    for phase, view in enumerate(sent):
+        take(view, send.at[phase])
 
 
 def write_out(result, new_state, result_out, state_out, sem):
@@ -455,13 +408,11 @@
         V((NEP, 8, 128), BF16), V((NTP, NEP, 8, 128), BF16), V((NZ * PITCH, 128), F32), V((ROWS, D), BF16),
         V((ROWS, FE), BF16), V((NTP, ROWS, WIDTH), BF16), V((4, ROWS, WIDTH), BF16), V((4, ROWS, WIDTH), BF16),
         V((3, ROWS, WIDTH), BF16), V((NEP, 8, 128), BF16), V((NEP, 8, 128), BF16),
-        V((NTP, 8, 128), BF16), V((NEP, NTP, 8, 128), BF16), V((ROWS, D), BF16),
-        V((NX, CHUNKS, 32, D // CHUNKS), BF16), V((3, CHUNKS, 32, D // CHUNKS), BF16),
-        V((NZ, NTP, 8, 128), BF16), V((NZ - 1, NTP, 8, 128), BF16), V((NTP, 8, 128), BF16), V((NTP, 8, 128), BF16),
-        dma((22,)),
-        dma((7,)), dma, dma((7,)), dma, dma((7,)), dma, dma, dma, dma((7,)), dma((7,)), dma((3, 8)), dma((3, 8)),
-        dma((3,)), dma((3,)), dma((4,)), dma((4,)), dma((4,)), dma((4,)), dma((3,)), dma((3,)), dma, dma,
-        dma((3, CHUNKS)), dma((3, CHUNKS)), dma((7, CHUNKS)), dma((CHUNKS,)), dma((7,)), dma,
+        V((NTP, 8, 128), BF16), V((NEP, NTP, 8, 128), BF16), V((NX, SEQ, D), BF16),
+        V((NX, CHUNKS, SEQ, WIDE), BF16), V((NX - 1, CHUNKS, SEQ, WIDE), BF16),
+        V((NZ, NTP, 8, 128), BF16), V((NZ * NTP, 8, 128), BF16),
+        dma((22,)), dma((12,)), dma, dma, dma((NZ,)), dma((NZ,)), dma((3,)), dma((3,)), dma((4,)), dma((4,)), dma((3,)),
+        dma, dma((3, CHUNKS)), dma,
         pltpu.SemaphoreType.REGULAR((3,)),
     ]
     kept = (V((SEQ, WIDTH), BF16), V((SEQ, DK, DK), F32))

time: 54.4 us -> 52.2 us (0.960)
  Pallas kernels: 53.7 us -> 51.5 us
    pallas_call x1, Pallas kernels: 52.3 us -> 50.1 us  [per_device(): pl.pallas_call(kernel, out_shape=kept, in_specs=[pl.BlockSpec(memory_spac...]
where the time goes in v3:
time: 52.2 us; the launch traced here: 52.1 us
  Pallas kernels  51.5 us (99%)
  between operations  0.65 us (1%)
    pallas_call x1, Pallas kernels, per_device(): pl.pallas_call(kernel, out_shape=kept, in_specs=[pl.BlockSpec(memory_spac...  50.1 us
    pallas_call x1, Pallas kernels, per_device(): pl.pallas_call(write_out, out_shape=tuple((jax.ShapeDtypeStruct(k.shape,...  1.34 us

profile of v3, /device:TPU:1, one launch (start us, length us, event | category | flops | bytes accessed | tf_op | source)
XLA Modules:
  0.0 52.1 jit_solution(12901871404578680026)
XLA Ops:
  0.6 50.1 %shard_map.221 = (bf16[32,256]{1,0:T(8,128)(2,1)S(1)}, f32[32,128,128]{2,1,0:T(8,128)S(1)}) custom-call(bf16[32,256]{1,0:T(8,128)(2,1)} %hidden.1, f32[32,128,128]{2,1,0:T(8,128)} %bitcast.16, f32[1,2048]{1,0:T(1,128)} %bitcast.22, bf16[2048,128]{1,0:T(8,128)(2,1)} %wq.1, bf16[2048,128]{1,0:T(8,128)(2,1)} %wk.1, bf16[2048,128]{1,0:T(8,128)(2,1)} %wv.1, ...), custom_call_target="tpu_custom_call" | custom-call | tf_op jit(solution)/shard_map/pallas_call | solution.py:419
  50.8 1.3 %shard_map.222 = (bf16[32,256]{1,0:T(8,128)(2,1)}, f32[32,128,128]{2,1,0:T(8,128)}) custom-call(bf16[32,256]{1,0:T(8,128)(2,1)S(1)} %get-tuple-element.6.result, f32[32,128,128]{2,1,0:T(8,128)S(1)} %get-tuple-element.7.new_state), custom_call_target="tpu_custom_call" | custom-call | tf_op jit(solution)/shard_map/pallas_call | solution.py:429

commit v4 on v3

v4 whole, which is shorter than its diff:
```python
import functools

import jax
import jax.numpy as jnp
from jax import lax
from jax.experimental import pallas as pl
from jax.experimental.pallas import tpu as pltpu
from jax.sharding import PartitionSpec as P

EPS = 1e-06
MESH = pl.DeviceIdType.MESH
F32, BF16, I32 = jnp.float32, jnp.bfloat16, jnp.int32

NX, NZ, NTP, NEP = 4, 8, 8, 32
SEQ, D, WIDTH, DK, CAP = 32, 2048, 256, 128, 4
ROWS = NEP * CAP
FE, FD = 384, 128
PITCH = 72
CHUNKS = 4
WIDE = D // CHUNKS
FAR_TP = FAR_Z = (4, 3, 5, 2, 6, 1, 7)


def silu(v):
    return v * jax.nn.sigmoid(v)


def dot(a, b):
    return jnp.dot(a, b, preferred_element_type=F32)


def dot_t(a, b):
    return lax.dot_general(a, b, (((1,), (1,)), ((), ())), preferred_element_type=F32)


def t_dot(a, b):
    return lax.dot_general(a, b, (((0,), (0,)), ((), ())), preferred_element_type=F32)


def iota(shape, dim):
    return lax.broadcasted_iota(I32, shape, dim)


def kernel(
    hidden, state, attn_gain, wq, wk, wv, wg, w_beta, w_decay, decay_scale, head_gain, w_out, ffn_gain, ids, route,
    eg, eu, ed, dg, du, dd, mix,
    result, new_state,
    hid_all, v_state, v_again, v_w, v_wb, v_wd, v_dscale, v_hgain, v_wo, v_fgain, v_ids, v_route,
    v_e, v_ed, v_d, v_dd, v_mix,
    xn_a, heads_all, mixed_s, send_mat, take_mat,
    disp, xa, stage, xn_e, inner_s, pb, pr, qs, yr, ret, rb,
    own_tok, dx, xn_d, px, xr, zs, fr,
    l_sem, send, a_recv, h_recv, t_recv, d_recv, x_recv, y_recv, p_recv, q_recv, b_recv, u_recv, w_recv, met,
):
    ep = lax.axis_index("ep")
    t = lax.axis_index("tp")
    z, x = lax.div(ep, NX), lax.rem(ep, NX)
    y, c = lax.div(t, 2), lax.rem(t, 2)

    def tp_peer(d):
        return ep, lax.rem(t + d, NTP)

    def ep_peer(d):
        return lax.rem(ep + d, NEP), t

    def z_peer(d):
        return lax.rem(z + d, NZ) * NX + x, t

    def x_peer(d):
        return z * NX + lax.rem(x + d, NX), t

    def y_peer(d):
        return ep, lax.rem(y + d, 4) * 2 + c

    partner = (ep, y * 2 + 1 - c)

    def remote(src, dst, phase, recv, peer):
        pltpu.make_async_remote_copy(
            src_ref=src, dst_ref=dst, send_sem=send.at[phase], recv_sem=recv, device_id=peer, device_id_type=MESH
        ).start()

    def take(view, sem):
        pltpu.make_async_copy(view, view, sem).wait()

    barrier = pltpu.get_barrier_semaphore()
    near = [tp_peer(d) for d in range(1, NTP)] + [z_peer(1), z_peer(NZ - 1), x_peer(1), x_peer(NX - 1)]
    for peer in near:
        pl.semaphore_signal(barrier, inc=1, device_id=peer, device_id_type=MESH)

    def tell(number, peers):
        for peer in peers:
            pl.semaphore_signal(met.at[number], inc=1, device_id=peer, device_id_type=MESH)

    loads = {}
    pairs = (
        ("hid", (hidden,), hid_all.at[t]), ("again", (attn_gain,), v_again), ("w", (wq, wk, wv, wg), v_w),
        ("wb", (w_beta,), v_wb), ("wd", (w_decay,), v_wd), ("dscale", (decay_scale,), v_dscale),
        ("hgain", (head_gain,), v_hgain), ("ids", (ids,), v_ids), ("route", (route,), v_route),
        ("state", (state,), v_state), ("wo", (w_out,), v_wo), ("fgain", (ffn_gain,), v_fgain), ("mix", (mix,), v_mix),
        ("d", (dg, du), v_d), ("dd", (dd,), v_dd), ("e", (eg, eu), v_e), ("ed", (ed,), v_ed),
    )
    for number, (name, sources, dst) in enumerate(pairs):
        loads[name] = functools.partial(take, dst, l_sem.at[number])
        for place, src in enumerate(sources):
            part = dst.at[place] if len(sources) > 1 else dst
            pltpu.make_async_copy(src, part, l_sem.at[number]).start()

    loads["hid"]()
    pl.semaphore_wait(barrier, len(near))

    for d in FAR_TP:
        remote(hid_all.at[t], hid_all.at[t], 0, a_recv, tp_peer(d))
    tell(0, (z_peer(1), z_peer(NZ - 1), x_peer(1), x_peer(NX - 1)))
    loads["ids"]()
    loads["route"]()
    first, second = v_ids[0:1, :], v_ids[1:2, :]
    expert = iota((NEP, SEQ), 0)
    is_first, is_second = first == expert, second == expert
    chosen = jnp.where(is_first | is_second, 1.0, 0.0)
    earlier = jnp.where(iota((SEQ, SEQ), 0) < iota((SEQ, SEQ), 1), 1.0, 0.0).astype(BF16)
    before = dot(chosen.astype(BF16), earlier)
    place = (chosen * (before + 1.0)).astype(BF16)
    row = iota((NEP * 8, NEP), 0)
    spread = jnp.where(row // 8 == iota((NEP * 8, NEP), 1), 1.0, 0.0).astype(BF16)
    hit = dot(spread, place) == ((row % 8) // 2 + 1).astype(F32)
    weight = jnp.where(is_first, v_route[0:1, :], 0.0) + jnp.where(is_second, v_route[1:2, :], 0.0)
    coarse = weight.astype(BF16)
    fine = (weight - coarse.astype(F32)).astype(BF16)
    coarse, fine = dot(spread, coarse), dot(spread, fine)
    for h in range(2):
        here = hit & (row % 2 == h)
        send_mat[h, : NEP * 8] = jnp.where(here, 1.0, 0.0).astype(BF16)
        take_mat[2 * h] = jnp.where(here, coarse, 0.0).astype(BF16)
        take_mat[2 * h + 1] = jnp.where(here, fine, 0.0).astype(BF16)
    t_row, t_col = iota((NTP * 8, SEQ), 0), iota((NTP * 8, SEQ), 1)
    for h in range(2):
        send_mat[h, NEP * 8 :] = jnp.where((t_row // 2 == t_col) & (t_row % 2 == h), 1.0, 0.0).astype(BF16)

    pl.semaphore_wait(met.at[0], 4)
    tell(1, (z_peer(2), z_peer(NZ - 2)))
    loads["again"]()
    take(hid_all.at[pl.ds(0, 7)], a_recv)

    pl.semaphore_wait(met.at[1], 2)
    tell(2, (x_peer(1), x_peer(2), x_peer(3), z_peer(NZ // 2)))
    square = jnp.zeros((SEQ, WIDTH), F32)
    for b in range(NTP):
        wide = hid_all[b].astype(F32)
        square = square + wide * wide
    scale = lax.rsqrt(jnp.sum(square, axis=-1, keepdims=True) * (1.0 / D) + EPS)
    for b in range(NTP):
        cols = slice(b * WIDTH, (b + 1) * WIDTH)
        xn_a[:, cols] = (hid_all[b].astype(F32) * scale * v_again[:, cols]).astype(BF16)
    for name in ("w", "wb", "wd", "dscale", "hgain"):
        loads[name]()
    normed = xn_a[...]
    queries, keys, values, gates = (dot(normed, v_w[i]) for i in range(4))
    queries = queries * lax.rsqrt(jnp.sum(queries * queries, axis=-1, keepdims=True) + EPS) * DK ** (-0.5)
    keys = keys * lax.rsqrt(jnp.sum(keys * keys, axis=-1, keepdims=True) + EPS)
    mine = iota((SEQ, NTP), 1) == t
    beta = jax.nn.sigmoid(jnp.sum(jnp.where(mine, dot_t(normed, v_wb[...]), 0.0), axis=-1, keepdims=True))
    logit = jnp.sum(jnp.where(mine, dot_t(normed, v_wd[...]), 0.0), axis=-1, keepdims=True)
    d_scale = jnp.sum(jnp.where(iota((1, NTP), 1) == t, v_dscale[...], 0.0), axis=-1, keepdims=True)
    soft = jnp.maximum(logit, 0.0) + jnp.log(1.0 + jnp.exp(-jnp.abs(logit)))
    decay = jnp.exp(-d_scale * soft)

    loads["state"]()
    qb, kb = queries.astype(BF16), keys.astype(BF16)
    diag = iota((16, 1024), 1) // DK == iota((16, 1024), 0) % 8
    by_query, by_key = [], []
    for i in range(SEQ // 8):
        both = jnp.concatenate([qb[8 * i : 8 * i + 8].astype(F32), kb[8 * i : 8 * i + 8].astype(F32)], axis=0)
        lhs = jnp.where(diag, jnp.concatenate([both] * 8, axis=1), 0.0).astype(BF16)
        rhs = v_state[8 * i : 8 * i + 8].reshape(1024, DK).astype(BF16)
        out = dot(lhs, rhs)
        by_query.append(out[:8])
        by_key.append(out[8:])
    s_q = jnp.concatenate(by_query, axis=0)
    s_k = jnp.concatenate(by_key, axis=0)
    match = beta * jnp.sum(queries * keys, axis=-1, keepdims=True)
    read = decay * (s_q - match * s_k) + match * values
    read = read * lax.rsqrt(jnp.mean(read * read, axis=-1, keepdims=True) + EPS) * v_hgain[...]
    heads_all[t] = (read * silu(gates)).astype(BF16)
    for d in FAR_TP:
        remote(heads_all.at[t], heads_all.at[t], 1, h_recv, tp_peer(d))
    update = beta * (values - decay * s_k)
    keys_t = jnp.concatenate([keys, jnp.zeros((DK - SEQ, DK), F32)], axis=0).T
    decay_rows = jnp.broadcast_to(decay, (SEQ, DK))
    for s in range(SEQ):
        new_state[s] = decay_rows[s : s + 1] * v_state[s] + keys_t[:, s : s + 1] * update[s : s + 1]

    pl.semaphore_wait(met.at[2], 4)
    loads["wo"]()
    take(heads_all.at[pl.ds(0, 7)], h_recv)
    wide = hid_all[t].astype(F32)
    for b in range(NTP):
        wide = wide + dot(heads_all[b], v_wo[b * DK : (b + 1) * DK, :])
    mixed = wide.astype(BF16)
    mixed_s[...] = mixed
    low, high = mixed[:, :128], mixed[:, 128:]

    moved = (dot(send_mat[0], low) + dot(send_mat[1], high)).reshape(NEP + NTP, 8, 128).astype(BF16)
    disp[...] = moved[:NEP]
    own_tok[...] = moved[NEP:]
    for dz in FAR_Z + (0,):
        base = z_peer(dz)[0] - x
        for d in (2, 1, 3, 0):
            if dz or d:
                to = base + lax.rem(x + d, NX)
                remote(disp.at[to], xa.at[t, ep], 3, d_recv.at[dz], (to, t))
    xa[t, ep] = disp[ep]
    for dz in FAR_Z + (0,):
        for d in FAR_TP + (0,):
            if dz or d:
                to = lax.rem(t + d, NTP)
                remote(own_tok.at[to], dx.at[ep, t], 2, t_recv.at[dz], (z_peer(dz)[0], to))
    dx[ep, t] = own_tok[t]
    for dz in (0, 1, 7, 2, 6, 3, 5, 4):
        from_z = lax.rem(z + NZ - dz, NZ)
        take(disp.at[pl.ds(0, NX if dz else NX - 1)], d_recv.at[dz])
        block = xa.at[t, pl.ds(from_z * NX, NX)]
        for d in FAR_TP:
            remote(block, block, 5, y_recv, tp_peer(d))
        take(dx.at[0] if dz else dx.at[0, pl.ds(0, 7)], t_recv.at[dz])
        block = dx.at[from_z * NX + x]
        for d in (2, 1, 3):
            remote(block, block, 4, x_recv, x_peer(d))
    loads["fgain"]()
    for name in ("d", "dd"):
        loads[name]()

    def dense(first, last):
        for d in range(first, last):
            xx = lax.rem(x + NX - d, NX)
            for zz in range(NZ):
                stage[pl.ds(zz * PITCH, 64), :] = dx[zz * NX + xx].astype(F32).reshape(64, 128)
            square = [jnp.zeros((8, 128), F32) for _ in range(4)]
            for j in range(4):
                for b in range(16):
                    part = stage[pl.ds((b // 2) * 8 + j * 2 + b % 2, 8, stride=PITCH), :]
                    square[j] = square[j] + part * part
            scales = [lax.rsqrt(jnp.sum(sq, axis=-1, keepdims=True) * (1.0 / D) + EPS) for sq in square]
            for b in range(16):
                cols = slice(b * 128, (b + 1) * 128)
                parts = [
                    stage[pl.ds((b // 2) * 8 + j * 2 + b % 2, 8, stride=PITCH), :] * scales[j] * v_fgain[:, cols]
                    for j in range(4)
                ]
                xn_d[d * SEQ : (d + 1) * SEQ, cols] = jnp.concatenate(parts, axis=0).astype(BF16)
        rows = xn_d[first * SEQ : last * SEQ]
        hidden_d = (silu(dot(rows, v_d[0])) * dot(rows, v_d[1])).astype(BF16)
        for f in range(CHUNKS):
            out = dot(hidden_d, v_dd[:, f * WIDE : (f + 1) * WIDE]).astype(BF16)
            for d in range(first, last):
                px[d, f] = out[(d - first) * SEQ : (d - first + 1) * SEQ]
            for d in (2, 1, 3):
                if first <= d < last:
                    back = NX - d
                    remote(px.at[d, f], xr.at[back - 1, f], 6, u_recv.at[f], x_peer(back))

    dense(0, 1)
    take(dx.at[pl.ds(0, 24)], x_recv)
    dense(1, NX)
    for name in ("e", "ed"):
        loads[name]()
    take(xa.at[pl.ds(0, 7)], y_recv)
    square = jnp.zeros((ROWS, 128), F32)
    for b in range(NTP):
        stage[pl.ds(0, 256), :] = xa[b].astype(F32).reshape(256, 128)
        for h in range(2):
            part = stage[pl.ds(h, ROWS, stride=2), :]
            square = square + part * part
            xn_e[:, b * WIDTH + h * 128 : b * WIDTH + (h + 1) * 128] = part.astype(BF16)
    scale = lax.rsqrt(jnp.sum(square, axis=-1, keepdims=True) * (1.0 / D) + EPS)
    for b in range(NTP):
        cols = slice(b * WIDTH, (b + 1) * WIDTH)
        xn_e[:, cols] = (xn_e[:, cols].astype(F32) * scale * v_fgain[:, cols]).astype(BF16)
    rows_e = xn_e[...]
    inner_s[...] = (silu(dot(rows_e, v_e[0])) * dot(rows_e, v_e[1])).astype(BF16)
    inner = inner_s[...]
    for b in range(NTP):
        pb[b] = dot(inner, v_ed[:, b * WIDTH : (b + 1) * WIDTH]).astype(BF16)
    for d in (2, 1, 3, 0):
        there = lax.rem(y + d, 4)
        remote(pb.at[there * 2 + 1 - c], pr.at[there], 7, p_recv.at[d], partner)
    for d in (2, 1, 3, 0):
        there = lax.rem(y + d, 4)
        take(pr.at[0], p_recv.at[d])
        qs[there] = (pb[there * 2 + c].astype(F32) + pr[there].astype(F32)).astype(BF16)
        if d > 0:
            remote(qs.at[there], yr.at[d - 1], 8, q_recv.at[d - 1], y_peer(d))

    def sum_x(f):
        take(xr.at[:, f], u_recv.at[f])
        total = px[0, f].astype(F32)
        for d in range(3):
            total = total + xr[d, f].astype(F32)
        for tt in range(2):
            for h in range(2):
                cols = slice(tt * WIDTH + h * 128, tt * WIDTH + (h + 1) * 128)
                for j in range(4):
                    stage[pl.ds(tt * 8 + j * 2 + h, 8, stride=PITCH), :] = total[j * 8 : (j + 1) * 8, cols]
        for zz in range(NZ):
            zs[zz, 2 * f : 2 * f + 2] = stage[pl.ds(zz * PITCH, 16), :].reshape(2, 8, 128).astype(BF16)
        for dz in FAR_Z + (0,):
            to = z_peer(dz)[0]

            def piece(tt):
                remote(zs.at[lax.div(to, NX), tt], fr.at[z * NTP + t], 9, w_recv, (to, tt))

            for tt in (2 * f, 2 * f + 1):
                if dz:
                    piece(tt)
                else:
                    pl.when(t != tt)(functools.partial(piece, tt))

    sum_x(0)
    sum_x(1)
    sum_x(2)
    sum_x(3)
    fr[z * NTP + t] = zs[z, t]
    for d in (1, 3, 2):
        take(yr.at[0], q_recv.at[d - 1])
    total = qs[y].astype(F32)
    for d in range(3):
        total = total + yr[d].astype(F32)
    total = total.astype(BF16).astype(F32)
    for h in range(2):
        stage[pl.ds(h, ROWS, stride=2), :] = total[:, h * 128 : (h + 1) * 128]
    ret[...] = stage[pl.ds(0, 256), :].reshape(NEP, 8, 128).astype(BF16)

    for dz in FAR_Z + (0,):
        base = z_peer(dz)[0] - x
        for d in (2, 1, 3, 0):
            if dz or d:
                to = base + lax.rem(x + d, NX)
                remote(ret.at[to], rb.at[ep], 10, b_recv, (to, t))
    rb[ep] = ret[ep]
    loads["mix"]()
    take(fr.at[pl.ds(0, NZ * NTP - 1)], w_recv)
    total = fr[0:NTP].astype(F32)
    for zz in range(1, NZ):
        total = total + fr[zz * NTP : (zz + 1) * NTP].astype(F32)
    stage[pl.ds(0, 64), :] = total.reshape(64, 128)
    take(rb.at[pl.ds(0, NEP - 1)], b_recv)
    back = rb[...].astype(F32).reshape(NEP * 8, 128).astype(BF16)
    for h in range(2):
        cols = slice(h * 128, (h + 1) * 128)
        moe = t_dot(take_mat[2 * h], back) + t_dot(take_mat[2 * h + 1], back)
        dense_out = stage[pl.ds(h, SEQ, stride=2), :]
        result[:, cols] = (
            mixed_s[:, cols].astype(F32) + moe + jax.nn.sigmoid(v_mix[:, cols]) * dense_out
        ).astype(BF16)
    sent = (
        hid_all.at[pl.ds(0, 7)], heads_all.at[pl.ds(0, 7)], fr.at[pl.ds(0, 63)], disp.at[pl.ds(0, 31)],
        dx.at[pl.ds(0, 24)], xa.at[pl.ds(0, 7)], px.at[pl.ds(0, 3)], pb.at[pl.ds(0, 4)],
        qs.at[pl.ds(0, 3)], fr.at[pl.ds(0, 63)], ret.at[pl.ds(0, 31)],
    )
    for phase, view in enumerate(sent):
        take(view, send.at[phase])


def write_out(result, new_state, result_out, state_out, sem):
    first = pltpu.make_async_copy(new_state, state_out, sem.at[0])
    second = pltpu.make_async_copy(result, result_out, sem.at[1])
    first.start()
    second.start()
    first.wait()
    second.wait()


def per_device(
    hidden_in, state_in, attn_gain, w_query, w_key, w_value, w_gate, w_beta, w_decay, decay_scale, head_gain, w_output,
    ffn_gain, expert_ids, route_weight, expert_gate, expert_up, expert_down, dense_gate, dense_up, dense_down, dense_mix,
):
    operands = (
        hidden_in, state_in.reshape(SEQ, DK, DK), attn_gain.reshape(1, D), w_query, w_key, w_value, w_gate, w_beta.T,
        w_decay.T, decay_scale.reshape(1, NTP), head_gain.reshape(1, DK), w_output, ffn_gain.reshape(1, D), expert_ids.T,
        route_weight.T, expert_gate[0], expert_up[0], expert_down[0], dense_gate, dense_up, dense_down,
        dense_mix.reshape(1, WIDTH),
    )
    V = pltpu.VMEM
    vmem_of = [
        V((NTP, SEQ, WIDTH), BF16), V((SEQ, DK, DK), F32), V((1, D), F32), V((4, D, DK), BF16), V((NTP, D), BF16),
        V((NTP, D), BF16), V((1, NTP), F32), V((1, DK), F32), V((NTP * DK, WIDTH), BF16), V((1, D), F32),
        V((2, SEQ), I32), V((2, SEQ), F32), V((2, D, FE), BF16), V((FE, D), BF16), V((2, D, FD), BF16),
        V((FD, D), BF16), V((1, WIDTH), F32),
    ]
    dma = pltpu.SemaphoreType.DMA
    scratch = vmem_of + [
        V((SEQ, D), BF16), V((NTP, SEQ, DK), BF16), V((SEQ, WIDTH), BF16),
        V((2, (NEP + NTP) * 8, SEQ), BF16), V((4, NEP * 8, SEQ), BF16),
        V((NEP, 8, 128), BF16), V((NTP, NEP, 8, 128), BF16), V((NZ * PITCH, 128), F32), V((ROWS, D), BF16),
        V((ROWS, FE), BF16), V((NTP, ROWS, WIDTH), BF16), V((4, ROWS, WIDTH), BF16), V((4, ROWS, WIDTH), BF16),
        V((3, ROWS, WIDTH), BF16), V((NEP, 8, 128), BF16), V((NEP, 8, 128), BF16),
        V((NTP, 8, 128), BF16), V((NEP, NTP, 8, 128), BF16), V((NX * SEQ, D), BF16),
        V((NX, CHUNKS, SEQ, WIDE), BF16), V((NX - 1, CHUNKS, SEQ, WIDE), BF16),
        V((NZ, NTP, 8, 128), BF16), V((NZ * NTP, 8, 128), BF16),
        dma((17,)), dma((11,)), dma, dma, dma((NZ,)), dma((NZ,)), dma, dma, dma((4,)), dma((3,)),
        dma, dma((CHUNKS,)), dma,
        pltpu.SemaphoreType.REGULAR((3,)),
    ]
    kept = (V((SEQ, WIDTH), BF16), V((SEQ, DK, DK), F32))
    result, new_state = pl.pallas_call(
        kernel,
        out_shape=kept,
        in_specs=[pl.BlockSpec(memory_space=pltpu.HBM)] * len(operands),
        out_specs=tuple(pl.BlockSpec(memory_space=pltpu.VMEM) for _ in kept),
        scratch_shapes=scratch,
        compiler_params=pltpu.CompilerParams(
            collective_id=0, has_side_effects=True, vmem_limit_bytes=64000000
        ),
    )(*operands)
    result, new_state = pl.pallas_call(
        write_out,
        out_shape=tuple(jax.ShapeDtypeStruct(k.shape, k.dtype) for k in kept),
        in_specs=[pl.BlockSpec(memory_space=pltpu.VMEM)] * 2,
        out_specs=tuple(pl.BlockSpec(memory_space=pltpu.HBM) for _ in kept),
        scratch_shapes=[dma((2,))],
        compiler_params=pltpu.CompilerParams(vmem_limit_bytes=8 * 1024 * 1024),
    )(result, new_state)
    return result, new_state.reshape(state_in.shape)


def solution(mesh):
    return jax.shard_map(
        per_device,
        mesh=mesh,
        in_specs=(
            P("ep", "tp"), P("ep", "tp", None, None), P(), P(None, "tp"), P(None, "tp"), P(None, "tp"), P(None, "tp"),
            P(), P(), P(), P(), P(None, "tp"), P(), P("ep", None), P("ep", None), P("ep", None, "tp"),
            P("ep", None, "tp"), P("ep", "tp", None), P(None, "ep"), P(None, "ep"), P("ep", None), P("tp"),
        ),
        out_specs=(P("ep", "tp"), P("ep", "tp", None, None)),
        check_vma=False,
    )
```

time: 52.2 us -> 51.6 us (0.989)
  Pallas kernels: 51.5 us -> 50.8 us
    pallas_call x1, Pallas kernels: 50.1 us -> 49.4 us  [per_device(): pl.pallas_call(kernel, out_shape=kept, in_specs=[pl.BlockSpec(memory_spac...]
where the time goes in v4:
time: 51.6 us; the launch traced here: 51.4 us
  Pallas kernels  50.8 us (98%)
  between operations  0.65 us (1%)
    pallas_call x1, Pallas kernels, per_device(): pl.pallas_call(kernel, out_shape=kept, in_specs=[pl.BlockSpec(memory_spac...  49.4 us
    pallas_call x1, Pallas kernels, per_device(): pl.pallas_call(write_out, out_shape=tuple((jax.ShapeDtypeStruct(k.shape,...  1.34 us

profile of v4, /device:TPU:1, one launch (start us, length us, event | category | flops | bytes accessed | tf_op | source)
XLA Modules:
  0.0 51.4 jit_solution(8204219367355015892)
XLA Ops:
  0.6 49.4 %shard_map.221 = (bf16[32,256]{1,0:T(8,128)(2,1)S(1)}, f32[32,128,128]{2,1,0:T(8,128)S(1)}) custom-call(bf16[32,256]{1,0:T(8,128)(2,1)} %hidden.1, f32[32,128,128]{2,1,0:T(8,128)} %bitcast.16, f32[1,2048]{1,0:T(1,128)} %bitcast.22, bf16[2048,128]{1,0:T(8,128)(2,1)} %wq.1, bf16[2048,128]{1,0:T(8,128)(2,1)} %wk.1, bf16[2048,128]{1,0:T(8,128)(2,1)} %wv.1, ...), custom_call_target="tpu_custom_call" | custom-call | tf_op jit(solution)/shard_map/pallas_call | solution.py:404
  50.1 1.3 %shard_map.222 = (bf16[32,256]{1,0:T(8,128)(2,1)}, f32[32,128,128]{2,1,0:T(8,128)}) custom-call(bf16[32,256]{1,0:T(8,128)(2,1)S(1)} %get-tuple-element.6.result, f32[32,128,128]{2,1,0:T(8,128)S(1)} %get-tuple-element.7.new_state), custom_call_target="tpu_custom_call" | custom-call | tf_op jit(solution)/shard_map/pallas_call | solution.py:414

commit v5 on v4

--- a/solution.py
+++ b/solution.py
@@ -18,7 +18,10 @@
 PITCH = 72
 CHUNKS = 4
 WIDE = D // CHUNKS
+SENT = 7 * 8 + 7 * 4 + 63 + 31 + 24 * 8 + 3 * 32 + 4 * 32 + 12 * 16 + 4 * 32 + 3 * 32 + 63 + 31
 FAR_TP = FAR_Z = (4, 3, 5, 2, 6, 1, 7)
+NEAR_TP = (1, 7, 2, 6)
+ROUND_OF = (0, 1, 2, 3, 4, 3, 2, 1)
 
 
 def silu(v):
@@ -47,10 +50,10 @@
     result, new_state,
     hid_all, v_state, v_again, v_w, v_wb, v_wd, v_dscale, v_hgain, v_wo, v_fgain, v_ids, v_route,
     v_e, v_ed, v_d, v_dd, v_mix,
-    xn_a, heads_all, mixed_s, send_mat, take_mat,
-    disp, xa, stage, xn_e, inner_s, pb, pr, qs, yr, ret, rb,
-    own_tok, dx, xn_d, px, xr, zs, fr,
-    l_sem, send, a_recv, h_recv, t_recv, d_recv, x_recv, y_recv, p_recv, q_recv, b_recv, u_recv, w_recv, met,
+    heads_all, mixed_s, send_mat, take_mat,
+    disp, xa, stage, stage_e, square_e, acc_e, pb, pr, qs, yr, ret, rb,
+    own_tok, dx, xn_d, px, xr, zs, fr, count,
+    l_sem, send, a_recv, h_recv, t_recv, d_recv, x_recv, y_recv, c_recv, p_recv, q_recv, b_recv, u_recv, w_recv, met,
 ):
     ep = lax.axis_index("ep")
     t = lax.axis_index("tp")
@@ -74,9 +77,9 @@
 
     partner = (ep, y * 2 + 1 - c)
 
-    def remote(src, dst, phase, recv, peer):
+    def remote(src, dst, recv, peer):
         pltpu.make_async_remote_copy(
-            src_ref=src, dst_ref=dst, send_sem=send.at[phase], recv_sem=recv, device_id=peer, device_id_type=MESH
+            src_ref=src, dst_ref=dst, send_sem=send, recv_sem=recv, device_id=peer, device_id_type=MESH
         ).start()
 
     def take(view, sem):
@@ -109,7 +112,7 @@
     pl.semaphore_wait(barrier, len(near))
 
     for d in FAR_TP:
-        remote(hid_all.at[t], hid_all.at[t], 0, a_recv, tp_peer(d))
+        remote(hid_all.at[t], hid_all.at[t], a_recv.at[0 if d in NEAR_TP else 1], tp_peer(d))
     tell(0, (z_peer(1), z_peer(NZ - 1), x_peer(1), x_peer(NX - 1)))
     loads["ids"]()
     loads["route"]()
@@ -138,28 +141,36 @@
 
     pl.semaphore_wait(met.at[0], 4)
     tell(1, (z_peer(2), z_peer(NZ - 2)))
-    loads["again"]()
-    take(hid_all.at[pl.ds(0, 7)], a_recv)
-
+    for name in ("again", "w", "wb", "wd"):
+        loads[name]()
+
+    def project(slots):
+        sums = None
+        for b in slots:
+            cols = pl.ds(pl.multiple_of(b * WIDTH, WIDTH), WIDTH)
+            wide = hid_all[b].astype(F32)
+            part = (wide * v_again[b]).astype(BF16)
+            outs = [wide * wide] + [dot(part, v_w[i, cols, :]) for i in range(4)]
+            outs += [dot_t(part, v_wb[:, cols]), dot_t(part, v_wd[:, cols])]
+            sums = outs if sums is None else [total + out for total, out in zip(sums, outs)]
+        return sums
+
+    take(hid_all.at[pl.ds(0, 4)], a_recv.at[0])
+    sums = project([t] + [lax.rem(t + NTP - d, NTP) for d in NEAR_TP])
+    take(hid_all.at[pl.ds(0, 3)], a_recv.at[1])
+    late = project([lax.rem(t + NTP - d, NTP) for d in (3, 5, 4)])
+    sums = [total + part for total, part in zip(sums, late)]
     pl.semaphore_wait(met.at[1], 2)
     tell(2, (x_peer(1), x_peer(2), x_peer(3), z_peer(NZ // 2)))
-    square = jnp.zeros((SEQ, WIDTH), F32)
-    for b in range(NTP):
-        wide = hid_all[b].astype(F32)
-        square = square + wide * wide
-    scale = lax.rsqrt(jnp.sum(square, axis=-1, keepdims=True) * (1.0 / D) + EPS)
-    for b in range(NTP):
-        cols = slice(b * WIDTH, (b + 1) * WIDTH)
-        xn_a[:, cols] = (hid_all[b].astype(F32) * scale * v_again[:, cols]).astype(BF16)
-    for name in ("w", "wb", "wd", "dscale", "hgain"):
+    for name in ("dscale", "hgain"):
         loads[name]()
-    normed = xn_a[...]
-    queries, keys, values, gates = (dot(normed, v_w[i]) for i in range(4))
+    scale = lax.rsqrt(jnp.sum(sums[0], axis=-1, keepdims=True) * (1.0 / D) + EPS)
+    queries, keys, values, gates, beta_all, decay_all = (total * scale for total in sums[1:])
     queries = queries * lax.rsqrt(jnp.sum(queries * queries, axis=-1, keepdims=True) + EPS) * DK ** (-0.5)
     keys = keys * lax.rsqrt(jnp.sum(keys * keys, axis=-1, keepdims=True) + EPS)
     mine = iota((SEQ, NTP), 1) == t
-    beta = jax.nn.sigmoid(jnp.sum(jnp.where(mine, dot_t(normed, v_wb[...]), 0.0), axis=-1, keepdims=True))
-    logit = jnp.sum(jnp.where(mine, dot_t(normed, v_wd[...]), 0.0), axis=-1, keepdims=True)
+    beta = jax.nn.sigmoid(jnp.sum(jnp.where(mine, beta_all, 0.0), axis=-1, keepdims=True))
+    logit = jnp.sum(jnp.where(mine, decay_all, 0.0), axis=-1, keepdims=True)
     d_scale = jnp.sum(jnp.where(iota((1, NTP), 1) == t, v_dscale[...], 0.0), axis=-1, keepdims=True)
     soft = jnp.maximum(logit, 0.0) + jnp.log(1.0 + jnp.exp(-jnp.abs(logit)))
     decay = jnp.exp(-d_scale * soft)
@@ -182,7 +193,7 @@
     read = read * lax.rsqrt(jnp.mean(read * read, axis=-1, keepdims=True) + EPS) * v_hgain[...]
     heads_all[t] = (read * silu(gates)).astype(BF16)
     for d in FAR_TP:
-        remote(heads_all.at[t], heads_all.at[t], 1, h_recv, tp_peer(d))
+        remote(heads_all.at[t], heads_all.at[t], h_recv, tp_peer(d))
     update = beta * (values - decay * s_k)
     keys_t = jnp.concatenate([keys, jnp.zeros((DK - SEQ, DK), F32)], axis=0).T
     decay_rows = jnp.broadcast_to(decay, (SEQ, DK))
@@ -207,24 +218,28 @@
         for d in (2, 1, 3, 0):
             if dz or d:
                 to = base + lax.rem(x + d, NX)
-                remote(disp.at[to], xa.at[t, ep], 3, d_recv.at[dz], (to, t))
+                remote(disp.at[to], xa.at[t, ep], d_recv.at[ROUND_OF[dz]], (to, t))
     xa[t, ep] = disp[ep]
     for dz in FAR_Z + (0,):
         for d in FAR_TP + (0,):
             if dz or d:
                 to = lax.rem(t + d, NTP)
-                remote(own_tok.at[to], dx.at[ep, t], 2, t_recv.at[dz], (z_peer(dz)[0], to))
+                remote(own_tok.at[to], dx.at[ep, t], t_recv.at[ROUND_OF[dz]], (z_peer(dz)[0], to))
     dx[ep, t] = own_tok[t]
-    for dz in (0, 1, 7, 2, 6, 3, 5, 4):
-        from_z = lax.rem(z + NZ - dz, NZ)
-        take(disp.at[pl.ds(0, NX if dz else NX - 1)], d_recv.at[dz])
-        block = xa.at[t, pl.ds(from_z * NX, NX)]
-        for d in FAR_TP:
-            remote(block, block, 5, y_recv, tp_peer(d))
-        take(dx.at[0] if dz else dx.at[0, pl.ds(0, 7)], t_recv.at[dz])
-        block = dx.at[from_z * NX + x]
-        for d in (2, 1, 3):
-            remote(block, block, 4, x_recv, x_peer(d))
+    for distance in range(NZ // 2 + 1):
+        group = [dz for dz in range(NZ) if ROUND_OF[dz] == distance]
+        blocks = [lax.rem(z + NZ - dz, NZ) for dz in group]
+        take(disp.at[pl.ds(0, NX * len(group) if distance else NX - 1)], d_recv.at[distance])
+        for from_z in blocks:
+            block = xa.at[t, pl.ds(from_z * NX, NX)]
+            for d in (2, 1, 3):
+                remote(block, block, y_recv.at[d - 1], y_peer(d))
+            remote(block, block, c_recv.at[0], partner)
+        take(fr.at[pl.ds(0, NTP * len(group) if distance else NTP - 1)], t_recv.at[distance])
+        for from_z in blocks:
+            block = dx.at[from_z * NX + x]
+            for d in (2, 1, 3):
+                remote(block, block, x_recv, x_peer(d))
     loads["fgain"]()
     for name in ("d", "dd"):
         loads[name]()
@@ -243,7 +258,7 @@
             for b in range(16):
                 cols = slice(b * 128, (b + 1) * 128)
                 parts = [
-                    stage[pl.ds((b // 2) * 8 + j * 2 + b % 2, 8, stride=PITCH), :] * scales[j] * v_fgain[:, cols]
+                    stage[pl.ds((b // 2) * 8 + j * 2 + b % 2, 8, stride=PITCH), :] * scales[j] * v_fgain[b // 2, :, (b % 2) * 128 : (b % 2 + 1) * 128]
                     for j in range(4)
                 ]
                 xn_d[d * SEQ : (d + 1) * SEQ, cols] = jnp.concatenate(parts, axis=0).astype(BF16)
@@ -256,39 +271,51 @@
             for d in (2, 1, 3):
                 if first <= d < last:
                     back = NX - d
-                    remote(px.at[d, f], xr.at[back - 1, f], 6, u_recv.at[f], x_peer(back))
+                    remote(px.at[d, f], xr.at[back - 1, f], u_recv.at[f], x_peer(back))
 
     dense(0, 1)
-    take(dx.at[pl.ds(0, 24)], x_recv)
-    dense(1, NX)
     for name in ("e", "ed"):
         loads[name]()
-    take(xa.at[pl.ds(0, 7)], y_recv)
-    square = jnp.zeros((ROWS, 128), F32)
-    for b in range(NTP):
-        stage[pl.ds(0, 256), :] = xa[b].astype(F32).reshape(256, 128)
-        for h in range(2):
-            part = stage[pl.ds(h, ROWS, stride=2), :]
-            square = square + part * part
-            xn_e[:, b * WIDTH + h * 128 : b * WIDTH + (h + 1) * 128] = part.astype(BF16)
-    scale = lax.rsqrt(jnp.sum(square, axis=-1, keepdims=True) * (1.0 / D) + EPS)
-    for b in range(NTP):
-        cols = slice(b * WIDTH, (b + 1) * WIDTH)
-        xn_e[:, cols] = (xn_e[:, cols].astype(F32) * scale * v_fgain[:, cols]).astype(BF16)
-    rows_e = xn_e[...]
-    inner_s[...] = (silu(dot(rows_e, v_e[0])) * dot(rows_e, v_e[1])).astype(BF16)
-    inner = inner_s[...]
+
+    def expert_slices(slots, start):
+        square, outs = 0.0, [0.0, 0.0]
+        for number, b in enumerate(slots):
+            base = pl.multiple_of(b * WIDTH, WIDTH)
+            stage_e[number] = xa[b].astype(F32).reshape(256, 128)
+            parts = [stage_e[number, pl.ds(h, ROWS, stride=2), :] for h in range(2)]
+            square = square + parts[0] * parts[0] + parts[1] * parts[1]
+            gain = v_fgain[b]
+            rows = jnp.concatenate([parts[h] * gain[:, h * 128 : (h + 1) * 128] for h in range(2)], axis=1).astype(BF16)
+            outs = [outs[i] + dot(rows, v_e[i, pl.ds(base, WIDTH), :]) for i in range(2)]
+        square_e[...] = square if start else square_e[...] + square
+        for i in range(2):
+            acc_e[i] = outs[i] if start else acc_e[i] + outs[i]
+
+    expert_slices([t], True)
+    take(xa.at[0], c_recv.at[0])
+    expert_slices([y * 2 + 1 - c], False)
+    for d in (1, 3, 2):
+        take(xa.at[0], y_recv.at[d - 1])
+        block = xa.at[lax.rem(y + 4 - d, 4) * 2 + c]
+        remote(block, block, c_recv.at[1], partner)
+    expert_slices([lax.rem(y + 4 - d, 4) * 2 + c for d in (1, 3, 2)], False)
+    take(xa.at[pl.ds(0, 3)], c_recv.at[1])
+    expert_slices([lax.rem(y + 4 - d, 4) * 2 + 1 - c for d in (1, 3, 2)], False)
+    scale = lax.rsqrt(jnp.sum(square_e[...], axis=-1, keepdims=True) * (1.0 / D) + EPS)
+    inner = (silu(acc_e[0] * scale) * (acc_e[1] * scale)).astype(BF16)
     for b in range(NTP):
         pb[b] = dot(inner, v_ed[:, b * WIDTH : (b + 1) * WIDTH]).astype(BF16)
     for d in (2, 1, 3, 0):
         there = lax.rem(y + d, 4)
-        remote(pb.at[there * 2 + 1 - c], pr.at[there], 7, p_recv.at[d], partner)
+        remote(pb.at[there * 2 + 1 - c], pr.at[there], p_recv.at[d], partner)
+    take(dx.at[pl.ds(0, 24)], x_recv)
+    dense(1, NX)
     for d in (2, 1, 3, 0):
         there = lax.rem(y + d, 4)
         take(pr.at[0], p_recv.at[d])
         qs[there] = (pb[there * 2 + c].astype(F32) + pr[there].astype(F32)).astype(BF16)
         if d > 0:
-            remote(qs.at[there], yr.at[d - 1], 8, q_recv.at[d - 1], y_peer(d))
+            remote(qs.at[there], yr.at[d - 1], q_recv.at[d - 1], y_peer(d))
 
     def sum_x(f):
         take(xr.at[:, f], u_recv.at[f])
@@ -306,7 +333,7 @@
             to = z_peer(dz)[0]
 
             def piece(tt):
-                remote(zs.at[lax.div(to, NX), tt], fr.at[z * NTP + t], 9, w_recv, (to, tt))
+                remote(zs.at[lax.div(to, NX), tt], fr.at[z * NTP + t], w_recv, (to, tt))
 
             for tt in (2 * f, 2 * f + 1):
                 if dz:
@@ -316,9 +343,6 @@
 
     sum_x(0)
     sum_x(1)
-    sum_x(2)
-    sum_x(3)
-    fr[z * NTP + t] = zs[z, t]
     for d in (1, 3, 2):
         take(yr.at[0], q_recv.at[d - 1])
     total = qs[y].astype(F32)
@@ -334,8 +358,11 @@
         for d in (2, 1, 3, 0):
             if dz or d:
                 to = base + lax.rem(x + d, NX)
-                remote(ret.at[to], rb.at[ep], 10, b_recv, (to, t))
+                remote(ret.at[to], rb.at[ep], b_recv, (to, t))
     rb[ep] = ret[ep]
+    sum_x(2)
+    sum_x(3)
+    fr[z * NTP + t] = zs[z, t]
     loads["mix"]()
     take(fr.at[pl.ds(0, NZ * NTP - 1)], w_recv)
     total = fr[0:NTP].astype(F32)
@@ -351,13 +378,7 @@
         result[:, cols] = (
             mixed_s[:, cols].astype(F32) + moe + jax.nn.sigmoid(v_mix[:, cols]) * dense_out
         ).astype(BF16)
-    sent = (
-        hid_all.at[pl.ds(0, 7)], heads_all.at[pl.ds(0, 7)], fr.at[pl.ds(0, 63)], disp.at[pl.ds(0, 31)],
-        dx.at[pl.ds(0, 24)], xa.at[pl.ds(0, 7)], px.at[pl.ds(0, 3)], pb.at[pl.ds(0, 4)],
-        qs.at[pl.ds(0, 3)], fr.at[pl.ds(0, 63)], ret.at[pl.ds(0, 31)],
-    )
-    for phase, view in enumerate(sent):
-        take(view, send.at[phase])
+    take(count, send)
 
 
 def write_out(result, new_state, result_out, state_out, sem):
@@ -374,29 +395,29 @@
     ffn_gain, expert_ids, route_weight, expert_gate, expert_up, expert_down, dense_gate, dense_up, dense_down, dense_mix,
 ):
     operands = (
-        hidden_in, state_in.reshape(SEQ, DK, DK), attn_gain.reshape(1, D), w_query, w_key, w_value, w_gate, w_beta.T,
-        w_decay.T, decay_scale.reshape(1, NTP), head_gain.reshape(1, DK), w_output, ffn_gain.reshape(1, D), expert_ids.T,
+        hidden_in, state_in.reshape(SEQ, DK, DK), attn_gain.reshape(NTP, 1, WIDTH), w_query, w_key, w_value, w_gate, w_beta.T,
+        w_decay.T, decay_scale.reshape(1, NTP), head_gain.reshape(1, DK), w_output, ffn_gain.reshape(NTP, 1, WIDTH), expert_ids.T,
         route_weight.T, expert_gate[0], expert_up[0], expert_down[0], dense_gate, dense_up, dense_down,
         dense_mix.reshape(1, WIDTH),
     )
     V = pltpu.VMEM
     vmem_of = [
-        V((NTP, SEQ, WIDTH), BF16), V((SEQ, DK, DK), F32), V((1, D), F32), V((4, D, DK), BF16), V((NTP, D), BF16),
-        V((NTP, D), BF16), V((1, NTP), F32), V((1, DK), F32), V((NTP * DK, WIDTH), BF16), V((1, D), F32),
+        V((NTP, SEQ, WIDTH), BF16), V((SEQ, DK, DK), F32), V((NTP, 1, WIDTH), F32), V((4, D, DK), BF16), V((NTP, D), BF16),
+        V((NTP, D), BF16), V((1, NTP), F32), V((1, DK), F32), V((NTP * DK, WIDTH), BF16), V((NTP, 1, WIDTH), F32),
         V((2, SEQ), I32), V((2, SEQ), F32), V((2, D, FE), BF16), V((FE, D), BF16), V((2, D, FD), BF16),
         V((FD, D), BF16), V((1, WIDTH), F32),
     ]
     dma = pltpu.SemaphoreType.DMA
     scratch = vmem_of + [
-        V((SEQ, D), BF16), V((NTP, SEQ, DK), BF16), V((SEQ, WIDTH), BF16),
+        V((NTP, SEQ, DK), BF16), V((SEQ, WIDTH), BF16),
         V((2, (NEP + NTP) * 8, SEQ), BF16), V((4, NEP * 8, SEQ), BF16),
-        V((NEP, 8, 128), BF16), V((NTP, NEP, 8, 128), BF16), V((NZ * PITCH, 128), F32), V((ROWS, D), BF16),
-        V((ROWS, FE), BF16), V((NTP, ROWS, WIDTH), BF16), V((4, ROWS, WIDTH), BF16), V((4, ROWS, WIDTH), BF16),
+        V((NEP, 8, 128), BF16), V((NTP, NEP, 8, 128), BF16), V((NZ * PITCH, 128), F32), V((3, 256, 128), F32),
+        V((ROWS, 128), F32), V((2, ROWS, FE), F32), V((NTP, ROWS, WIDTH), BF16), V((4, ROWS, WIDTH), BF16), V((4, ROWS, WIDTH), BF16),
         V((3, ROWS, WIDTH), BF16), V((NEP, 8, 128), BF16), V((NEP, 8, 128), BF16),
         V((NTP, 8, 128), BF16), V((NEP, NTP, 8, 128), BF16), V((NX * SEQ, D), BF16),
         V((NX, CHUNKS, SEQ, WIDE), BF16), V((NX - 1, CHUNKS, SEQ, WIDE), BF16),
-        V((NZ, NTP, 8, 128), BF16), V((NZ * NTP, 8, 128), BF16),
-        dma((17,)), dma((11,)), dma, dma, dma((NZ,)), dma((NZ,)), dma, dma, dma((4,)), dma((3,)),
+        V((NZ, NTP, 8, 128), BF16), V((NZ * NTP, 8, 128), BF16), V((SENT, 8, 128), BF16),
+        dma((17,)), dma, dma((2,)), dma, dma((5,)), dma((5,)), dma, dma((3,)), dma((2,)), dma((4,)), dma((3,)),
         dma, dma((CHUNKS,)), dma,
         pltpu.SemaphoreType.REGULAR((3,)),
     ]

time: 51.6 us -> 48.3 us (0.936)
  the two profiles are of different devices: /device:TPU:1 before, /device:TPU:25 now
where the time goes in v5:
time: 48.3 us; the launch traced here: 48.1 us
  Pallas kernels  47.5 us (98%)
  between operations  0.65 us (1%)
    pallas_call x1, Pallas kernels, per_device(): pl.pallas_call(kernel, out_shape=kept, in_specs=[pl.BlockSpec(memory_spac...  46.1 us
    pallas_call x1, Pallas kernels, per_device(): pl.pallas_call(write_out, out_shape=tuple((jax.ShapeDtypeStruct(k.shape,...  1.34 us

profile of v5, /device:TPU:25, one launch (start us, length us, event | category | flops | bytes accessed | tf_op | source)
XLA Modules:
  0.0 48.1 jit_solution(9038239679570240222)
XLA Ops:
  0.6 46.1 %shard_map.221 = (bf16[32,256]{1,0:T(8,128)(2,1)S(1)}, f32[32,128,128]{2,1,0:T(8,128)S(1)}) custom-call(bf16[32,256]{1,0:T(8,128)(2,1)} %hidden.1, f32[32,128,128]{2,1,0:T(8,128)} %bitcast.16, f32[8,1,256]{2,1,0:T(1,128)} %bitcast.22, bf16[2048,128]{1,0:T(8,128)(2,1)} %wq.1, bf16[2048,128]{1,0:T(8,128)(2,1)} %wk.1, bf16[2048,128]{1,0:T(8,128)(2,1)} %wv.1, ...), custom_call_target="tpu_custom_call" | custom-call | tf_op jit(solution)/shard_map/pallas_call | solution.py:425
  46.8 1.3 %shard_map.222 = (bf16[32,256]{1,0:T(8,128)(2,1)}, f32[32,128,128]{2,1,0:T(8,128)}) custom-call(bf16[32,256]{1,0:T(8,128)(2,1)S(1)} %get-tuple-element.6.result, f32[32,128,128]{2,1,0:T(8,128)S(1)} %get-tuple-element.7.new_state), custom_call_target="tpu_custom_call" | custom-call | tf_op jit(solution)/shard_map/pallas_call | solution.py:435

commit v6 on v5

--- a/solution.py
+++ b/solution.py
@@ -22,6 +22,7 @@
 FAR_TP = FAR_Z = (4, 3, 5, 2, 6, 1, 7)
 NEAR_TP = (1, 7, 2, 6)
 ROUND_OF = (0, 1, 2, 3, 4, 3, 2, 1)
+HALVES = ((0, 1, 7, 2), (6, 3, 5, 4))
 
 
 def silu(v):
@@ -52,7 +53,7 @@
     v_e, v_ed, v_d, v_dd, v_mix,
     heads_all, mixed_s, send_mat, take_mat,
     disp, xa, stage, stage_e, square_e, acc_e, pb, pr, qs, yr, ret, rb,
-    own_tok, dx, xn_d, px, xr, zs, fr, count,
+    own_tok, dx, xn_d, px, xr, sums_x, zs, fr, count,
     l_sem, send, a_recv, h_recv, t_recv, d_recv, x_recv, y_recv, c_recv, p_recv, q_recv, b_recv, u_recv, w_recv, met,
 ):
     ep = lax.axis_index("ep")
@@ -236,44 +237,44 @@
                 remote(block, block, y_recv.at[d - 1], y_peer(d))
             remote(block, block, c_recv.at[0], partner)
         take(fr.at[pl.ds(0, NTP * len(group) if distance else NTP - 1)], t_recv.at[distance])
-        for from_z in blocks:
+        for dz, from_z in zip(group, blocks):
             block = dx.at[from_z * NX + x]
             for d in (2, 1, 3):
-                remote(block, block, x_recv, x_peer(d))
+                remote(block, block, x_recv.at[int(dz in HALVES[1])], x_peer(d))
     loads["fgain"]()
     for name in ("d", "dd"):
         loads[name]()
 
-    def dense(first, last):
-        for d in range(first, last):
+    def dense(half):
+        take(dx.at[pl.ds(0, 12)], x_recv.at[half])
+        for d in range(NX):
             xx = lax.rem(x + NX - d, NX)
-            for zz in range(NZ):
-                stage[pl.ds(zz * PITCH, 64), :] = dx[zz * NX + xx].astype(F32).reshape(64, 128)
-            square = [jnp.zeros((8, 128), F32) for _ in range(4)]
+            for k, dz in enumerate(HALVES[half]):
+                block = dx[lax.rem(z + NZ - dz, NZ) * NX + xx]
+                stage[pl.ds((d * 4 + k) * PITCH, 64), :] = block.astype(F32).reshape(64, 128)
+            parts = [
+                [stage[pl.ds(d * 4 * PITCH + (b // 2) * 8 + j * 2 + b % 2, 4, stride=PITCH), :] for b in range(16)]
+                for j in range(4)
+            ]
             for j in range(4):
+                square = parts[j][0] * parts[j][0]
+                for b in range(1, 16):
+                    square = square + parts[j][b] * parts[j][b]
+                scale = lax.rsqrt(jnp.sum(square, axis=-1, keepdims=True) * (1.0 / D) + EPS)
+                row = d * 16 + j * 4
                 for b in range(16):
-                    part = stage[pl.ds((b // 2) * 8 + j * 2 + b % 2, 8, stride=PITCH), :]
-                    square[j] = square[j] + part * part
-            scales = [lax.rsqrt(jnp.sum(sq, axis=-1, keepdims=True) * (1.0 / D) + EPS) for sq in square]
-            for b in range(16):
-                cols = slice(b * 128, (b + 1) * 128)
-                parts = [
-                    stage[pl.ds((b // 2) * 8 + j * 2 + b % 2, 8, stride=PITCH), :] * scales[j] * v_fgain[b // 2, :, (b % 2) * 128 : (b % 2 + 1) * 128]
-                    for j in range(4)
-                ]
-                xn_d[d * SEQ : (d + 1) * SEQ, cols] = jnp.concatenate(parts, axis=0).astype(BF16)
-        rows = xn_d[first * SEQ : last * SEQ]
+                    gain = v_fgain[b // 2, :, (b % 2) * 128 : (b % 2 + 1) * 128]
+                    xn_d[row : row + 4, b * 128 : (b + 1) * 128] = parts[j][b] * scale * gain
+        rows = xn_d[...].astype(BF16)
         hidden_d = (silu(dot(rows, v_d[0])) * dot(rows, v_d[1])).astype(BF16)
         for f in range(CHUNKS):
             out = dot(hidden_d, v_dd[:, f * WIDE : (f + 1) * WIDE]).astype(BF16)
-            for d in range(first, last):
-                px[d, f] = out[(d - first) * SEQ : (d - first + 1) * SEQ]
+            for d in range(NX):
+                px[half, d, f] = out[d * 16 : (d + 1) * 16]
             for d in (2, 1, 3):
-                if first <= d < last:
-                    back = NX - d
-                    remote(px.at[d, f], xr.at[back - 1, f], u_recv.at[f], x_peer(back))
-
-    dense(0, 1)
+                back = NX - d
+                remote(px.at[half, d, f], xr.at[half, back - 1, f], u_recv.at[half, f], x_peer(back))
+
     for name in ("e", "ed"):
         loads[name]()
 
@@ -299,6 +300,7 @@
         block = xa.at[lax.rem(y + 4 - d, 4) * 2 + c]
         remote(block, block, c_recv.at[1], partner)
     expert_slices([lax.rem(y + 4 - d, 4) * 2 + c for d in (1, 3, 2)], False)
+    dense(0)
     take(xa.at[pl.ds(0, 3)], c_recv.at[1])
     expert_slices([lax.rem(y + 4 - d, 4) * 2 + 1 - c for d in (1, 3, 2)], False)
     scale = lax.rsqrt(jnp.sum(square_e[...], axis=-1, keepdims=True) * (1.0 / D) + EPS)
@@ -308,8 +310,7 @@
     for d in (2, 1, 3, 0):
         there = lax.rem(y + d, 4)
         remote(pb.at[there * 2 + 1 - c], pr.at[there], p_recv.at[d], partner)
-    take(dx.at[pl.ds(0, 24)], x_recv)
-    dense(1, NX)
+    dense(1)
     for d in (2, 1, 3, 0):
         there = lax.rem(y + d, 4)
         take(pr.at[0], p_recv.at[d])
@@ -317,23 +318,24 @@
         if d > 0:
             remote(qs.at[there], yr.at[d - 1], q_recv.at[d - 1], y_peer(d))
 
-    def sum_x(f):
-        take(xr.at[:, f], u_recv.at[f])
-        total = px[0, f].astype(F32)
+    def sum_x(half, f):
+        take(xr.at[half, :, f], u_recv.at[half, f])
+        total = px[half, 0, f].astype(F32)
         for d in range(3):
-            total = total + xr[d, f].astype(F32)
+            total = total + xr[half, d, f].astype(F32)
+        sums_x[...] = total
         for tt in range(2):
             for h in range(2):
                 cols = slice(tt * WIDTH + h * 128, tt * WIDTH + (h + 1) * 128)
                 for j in range(4):
-                    stage[pl.ds(tt * 8 + j * 2 + h, 8, stride=PITCH), :] = total[j * 8 : (j + 1) * 8, cols]
-        for zz in range(NZ):
-            zs[zz, 2 * f : 2 * f + 2] = stage[pl.ds(zz * PITCH, 16), :].reshape(2, 8, 128).astype(BF16)
-        for dz in FAR_Z + (0,):
-            to = z_peer(dz)[0]
+                    stage[pl.ds(tt * 8 + j * 2 + h, 4, stride=PITCH), :] = sums_x[j * 4 : (j + 1) * 4, cols]
+        for k, dz in enumerate(HALVES[half]):
+            zs[half * 4 + k, 2 * f : 2 * f + 2] = stage[pl.ds(k * PITCH, 16), :].reshape(2, 8, 128).astype(BF16)
+        for k, dz in reversed(tuple(enumerate(HALVES[half]))):
+            to = z_peer(NZ - dz)[0]
 
             def piece(tt):
-                remote(zs.at[lax.div(to, NX), tt], fr.at[z * NTP + t], w_recv, (to, tt))
+                remote(zs.at[half * 4 + k, tt], fr.at[z * NTP + t], w_recv, (to, tt))
 
             for tt in (2 * f, 2 * f + 1):
                 if dz:
@@ -341,8 +343,13 @@
                 else:
                     pl.when(t != tt)(functools.partial(piece, tt))
 
-    sum_x(0)
-    sum_x(1)
+    for f in range(CHUNKS):
+        sum_x(0, f)
+    sum_x(1, 0)
+    sum_x(1, 1)
+    sum_x(1, 2)
+    sum_x(1, 3)
+    fr[z * NTP + t] = zs[0, t]
     for d in (1, 3, 2):
         take(yr.at[0], q_recv.at[d - 1])
     total = qs[y].astype(F32)
@@ -360,9 +367,6 @@
                 to = base + lax.rem(x + d, NX)
                 remote(ret.at[to], rb.at[ep], b_recv, (to, t))
     rb[ep] = ret[ep]
-    sum_x(2)
-    sum_x(3)
-    fr[z * NTP + t] = zs[z, t]
     loads["mix"]()
     take(fr.at[pl.ds(0, NZ * NTP - 1)], w_recv)
     total = fr[0:NTP].astype(F32)
@@ -411,14 +415,14 @@
     scratch = vmem_of + [
         V((NTP, SEQ, DK), BF16), V((SEQ, WIDTH), BF16),
         V((2, (NEP + NTP) * 8, SEQ), BF16), V((4, NEP * 8, SEQ), BF16),
-        V((NEP, 8, 128), BF16), V((NTP, NEP, 8, 128), BF16), V((NZ * PITCH, 128), F32), V((3, 256, 128), F32),
+        V((NEP, 8, 128), BF16), V((NTP, NEP, 8, 128), BF16), V((16 * PITCH, 128), F32), V((3, 256, 128), F32),
         V((ROWS, 128), F32), V((2, ROWS, FE), F32), V((NTP, ROWS, WIDTH), BF16), V((4, ROWS, WIDTH), BF16), V((4, ROWS, WIDTH), BF16),
         V((3, ROWS, WIDTH), BF16), V((NEP, 8, 128), BF16), V((NEP, 8, 128), BF16),
-        V((NTP, 8, 128), BF16), V((NEP, NTP, 8, 128), BF16), V((NX * SEQ, D), BF16),
-        V((NX, CHUNKS, SEQ, WIDE), BF16), V((NX - 1, CHUNKS, SEQ, WIDE), BF16),
+        V((NTP, 8, 128), BF16), V((NEP, NTP, 8, 128), BF16), V((NX * 16, D), F32),
+        V((2, NX, CHUNKS, 16, WIDE), BF16), V((2, NX - 1, CHUNKS, 16, WIDE), BF16), V((16, WIDE), F32),
         V((NZ, NTP, 8, 128), BF16), V((NZ * NTP, 8, 128), BF16), V((SENT, 8, 128), BF16),
-        dma((17,)), dma, dma((2,)), dma, dma((5,)), dma((5,)), dma, dma((3,)), dma((2,)), dma((4,)), dma((3,)),
-        dma, dma((CHUNKS,)), dma,
+        dma((17,)), dma, dma((2,)), dma, dma((5,)), dma((5,)), dma((2,)), dma((3,)), dma((2,)), dma((4,)), dma((3,)),
+        dma, dma((2, CHUNKS)), dma,
         pltpu.SemaphoreType.REGULAR((3,)),
     ]
     kept = (V((SEQ, WIDTH), BF16), V((SEQ, DK, DK), F32))

time: 48.3 us -> 47.9 us (level)
  the two profiles are of different devices: /device:TPU:25 before, /device:TPU:1 now
where the time goes in v6:
time: 47.9 us; the launch traced here: 47.7 us
  Pallas kernels  47.1 us (98%)
  between operations  0.65 us (1%)
    pallas_call x1, Pallas kernels, per_device(): pl.pallas_call(kernel, out_shape=kept, in_specs=[pl.BlockSpec(memory_spac...  45.7 us
    pallas_call x1, Pallas kernels, per_device(): pl.pallas_call(write_out, out_shape=tuple((jax.ShapeDtypeStruct(k.shape,...  1.34 us

profile of v6, /device:TPU:1, one launch (start us, length us, event | category | flops | bytes accessed | tf_op | source)
XLA Modules:
  0.0 47.7 jit_solution(11079424251361572968)
XLA Ops:
  0.6 45.7 %shard_map.221 = (bf16[32,256]{1,0:T(8,128)(2,1)S(1)}, f32[32,128,128]{2,1,0:T(8,128)S(1)}) custom-call(bf16[32,256]{1,0:T(8,128)(2,1)} %hidden.1, f32[32,128,128]{2,1,0:T(8,128)} %bitcast.16, f32[8,1,256]{2,1,0:T(1,128)} %bitcast.22, bf16[2048,128]{1,0:T(8,128)(2,1)} %wq.1, bf16[2048,128]{1,0:T(8,128)(2,1)} %wk.1, bf16[2048,128]{1,0:T(8,128)(2,1)} %wv.1, ...), custom_call_target="tpu_custom_call" | custom-call | tf_op jit(solution)/shard_map/pallas_call | solution.py:429
  46.4 1.3 %shard_map.222 = (bf16[32,256]{1,0:T(8,128)(2,1)}, f32[32,128,128]{2,1,0:T(8,128)}) custom-call(bf16[32,256]{1,0:T(8,128)(2,1)S(1)} %get-tuple-element.6.result, f32[32,128,128]{2,1,0:T(8,128)S(1)} %get-tuple-element.7.new_state), custom_call_target="tpu_custom_call" | custom-call | tf_op jit(solution)/shard_map/pallas_call | solution.py:439

commit v7 on v6

--- a/solution.py
+++ b/solution.py
@@ -53,7 +53,7 @@
     v_e, v_ed, v_d, v_dd, v_mix,
     heads_all, mixed_s, send_mat, take_mat,
     disp, xa, stage, stage_e, square_e, acc_e, pb, pr, qs, yr, ret, rb,
-    own_tok, dx, xn_d, px, xr, sums_x, zs, fr, count,
+    own_tok, dx, xn_d, square_d, px, xr, sums_x, zs, fr, count,
     l_sem, send, a_recv, h_recv, t_recv, d_recv, x_recv, y_recv, c_recv, p_recv, q_recv, b_recv, u_recv, w_recv, met,
 ):
     ep = lax.axis_index("ep")
@@ -101,7 +101,7 @@
         ("wb", (w_beta,), v_wb), ("wd", (w_decay,), v_wd), ("dscale", (decay_scale,), v_dscale),
         ("hgain", (head_gain,), v_hgain), ("ids", (ids,), v_ids), ("route", (route,), v_route),
         ("state", (state,), v_state), ("wo", (w_out,), v_wo), ("fgain", (ffn_gain,), v_fgain), ("mix", (mix,), v_mix),
-        ("d", (dg, du), v_d), ("dd", (dd,), v_dd), ("e", (eg, eu), v_e), ("ed", (ed,), v_ed),
+        ("d", (dg, du), v_d), ("dd", (dd,), v_dd), ("e", (eg, eu), v_e), ("ed", tuple(ed.at[:, pl.ds(b * WIDTH, WIDTH)] for b in range(NTP)), v_ed),
     )
     for number, (name, sources, dst) in enumerate(pairs):
         loads[name] = functools.partial(take, dst, l_sem.at[number])
@@ -245,36 +245,39 @@
     for name in ("d", "dd"):
         loads[name]()
 
+    def load_rows(half, d):
+        xx = lax.rem(x + NX - d, NX)
+        for k, dz in enumerate(HALVES[half]):
+            block = dx[lax.rem(z + NZ - dz, NZ) * NX + xx]
+            stage[pl.ds((d * 4 + k) * PITCH, 64), :] = block.astype(F32).reshape(64, 128)
+        for j in range(4):
+            row = d * 16 + j * 4
+            square = 0.0
+            for b in range(16):
+                part = stage[pl.ds(d * 4 * PITCH + (b // 2) * 8 + j * 2 + b % 2, 4, stride=PITCH), :]
+                square = square + part * part
+                gain = v_fgain[b // 2, :, (b % 2) * 128 : (b % 2 + 1) * 128]
+                xn_d[half, row : row + 4, b * 128 : (b + 1) * 128] = part * gain
+            square_d[half, row : row + 4] = square
+
     def dense(half):
         take(dx.at[pl.ds(0, 12)], x_recv.at[half])
-        for d in range(NX):
-            xx = lax.rem(x + NX - d, NX)
-            for k, dz in enumerate(HALVES[half]):
-                block = dx[lax.rem(z + NZ - dz, NZ) * NX + xx]
-                stage[pl.ds((d * 4 + k) * PITCH, 64), :] = block.astype(F32).reshape(64, 128)
-            parts = [
-                [stage[pl.ds(d * 4 * PITCH + (b // 2) * 8 + j * 2 + b % 2, 4, stride=PITCH), :] for b in range(16)]
-                for j in range(4)
-            ]
-            for j in range(4):
-                square = parts[j][0] * parts[j][0]
-                for b in range(1, 16):
-                    square = square + parts[j][b] * parts[j][b]
-                scale = lax.rsqrt(jnp.sum(square, axis=-1, keepdims=True) * (1.0 / D) + EPS)
-                row = d * 16 + j * 4
-                for b in range(16):
-                    gain = v_fgain[b // 2, :, (b % 2) * 128 : (b % 2 + 1) * 128]
-                    xn_d[row : row + 4, b * 128 : (b + 1) * 128] = parts[j][b] * scale * gain
-        rows = xn_d[...].astype(BF16)
-        hidden_d = (silu(dot(rows, v_d[0])) * dot(rows, v_d[1])).astype(BF16)
+        for d in (1, 3, 2):
+            load_rows(half, d)
+        rows = xn_d[half].astype(BF16)
+        scale = lax.rsqrt(jnp.sum(square_d[half], axis=-1, keepdims=True) * (1.0 / D) + EPS)
+        hidden_d = (silu(dot(rows, v_d[0]) * scale) * (dot(rows, v_d[1]) * scale)).astype(BF16)
         for f in range(CHUNKS):
             out = dot(hidden_d, v_dd[:, f * WIDE : (f + 1) * WIDE]).astype(BF16)
             for d in range(NX):
                 px[half, d, f] = out[d * 16 : (d + 1) * 16]
+        for f in range(CHUNKS):
             for d in (2, 1, 3):
                 back = NX - d
                 remote(px.at[half, d, f], xr.at[half, back - 1, f], u_recv.at[half, f], x_peer(back))
 
+    load_rows(0, 0)
+    load_rows(1, 0)
     for name in ("e", "ed"):
         loads[name]()
 
@@ -305,11 +308,17 @@
     expert_slices([lax.rem(y + 4 - d, 4) * 2 + 1 - c for d in (1, 3, 2)], False)
     scale = lax.rsqrt(jnp.sum(square_e[...], axis=-1, keepdims=True) * (1.0 / D) + EPS)
     inner = (silu(acc_e[0] * scale) * (acc_e[1] * scale)).astype(BF16)
-    for b in range(NTP):
-        pb[b] = dot(inner, v_ed[:, b * WIDTH : (b + 1) * WIDTH]).astype(BF16)
+
+    def down(core):
+        for d in (2, 1, 3, 0):
+            b = lax.rem(y + d, 4) * 2 + core
+            pb[b] = dot(inner, v_ed[b]).astype(BF16)
+
+    down(1 - c)
     for d in (2, 1, 3, 0):
         there = lax.rem(y + d, 4)
         remote(pb.at[there * 2 + 1 - c], pr.at[there], p_recv.at[d], partner)
+    down(c)
     dense(1)
     for d in (2, 1, 3, 0):
         there = lax.rem(y + d, 4)
@@ -408,7 +417,7 @@
     vmem_of = [
         V((NTP, SEQ, WIDTH), BF16), V((SEQ, DK, DK), F32), V((NTP, 1, WIDTH), F32), V((4, D, DK), BF16), V((NTP, D), BF16),
         V((NTP, D), BF16), V((1, NTP), F32), V((1, DK), F32), V((NTP * DK, WIDTH), BF16), V((NTP, 1, WIDTH), F32),
-        V((2, SEQ), I32), V((2, SEQ), F32), V((2, D, FE), BF16), V((FE, D), BF16), V((2, D, FD), BF16),
+        V((2, SEQ), I32), V((2, SEQ), F32), V((2, D, FE), BF16), V((NTP, FE, WIDTH), BF16), V((2, D, FD), BF16),
         V((FD, D), BF16), V((1, WIDTH), F32),
     ]
     dma = pltpu.SemaphoreType.DMA
@@ -418,7 +427,7 @@
         V((NEP, 8, 128), BF16), V((NTP, NEP, 8, 128), BF16), V((16 * PITCH, 128), F32), V((3, 256, 128), F32),
         V((ROWS, 128), F32), V((2, ROWS, FE), F32), V((NTP, ROWS, WIDTH), BF16), V((4, ROWS, WIDTH), BF16), V((4, ROWS, WIDTH), BF16),
         V((3, ROWS, WIDTH), BF16), V((NEP, 8, 128), BF16), V((NEP, 8, 128), BF16),
-        V((NTP, 8, 128), BF16), V((NEP, NTP, 8, 128), BF16), V((NX * 16, D), F32),
+        V((NTP, 8, 128), BF16), V((NEP, NTP, 8, 128), BF16), V((2, NX * 16, D), F32), V((2, NX * 16, 128), F32),
         V((2, NX, CHUNKS, 16, WIDE), BF16), V((2, NX - 1, CHUNKS, 16, WIDE), BF16), V((16, WIDE), F32),
         V((NZ, NTP, 8, 128), BF16), V((NZ * NTP, 8, 128), BF16), V((SENT, 8, 128), BF16),
         dma((17,)), dma, dma((2,)), dma, dma((5,)), dma((5,)), dma((2,)), dma((3,)), dma((2,)), dma((4,)), dma((3,)),

time: 47.9 us -> 47.1 us (0.983)
  Pallas kernels: 47.1 us -> 46.3 us
    pallas_call x1, Pallas kernels: 45.7 us -> 44.9 us  [per_device(): pl.pallas_call(kernel, out_shape=kept, in_specs=[pl.BlockSpec(memory_spac...]
where the time goes in v7:
time: 47.1 us; the launch traced here: 46.9 us
  Pallas kernels  46.3 us (98%)
  between operations  0.65 us (1%)
    pallas_call x1, Pallas kernels, per_device(): pl.pallas_call(kernel, out_shape=kept, in_specs=[pl.BlockSpec(memory_spac...  44.9 us
    pallas_call x1, Pallas kernels, per_device(): pl.pallas_call(write_out, out_shape=tuple((jax.ShapeDtypeStruct(k.shape,...  1.34 us

profile of v7, /device:TPU:1, one launch (start us, length us, event | category | flops | bytes accessed | tf_op | source)
XLA Modules:
  0.0 46.9 jit_solution(3970294749105253363)
XLA Ops:
  0.6 44.9 %shard_map.221 = (bf16[32,256]{1,0:T(8,128)(2,1)S(1)}, f32[32,128,128]{2,1,0:T(8,128)S(1)}) custom-call(bf16[32,256]{1,0:T(8,128)(2,1)} %hidden.1, f32[32,128,128]{2,1,0:T(8,128)} %bitcast.16, f32[8,1,256]{2,1,0:T(1,128)} %bitcast.22, bf16[2048,128]{1,0:T(8,128)(2,1)} %wq.1, bf16[2048,128]{1,0:T(8,128)(2,1)} %wk.1, bf16[2048,128]{1,0:T(8,128)(2,1)} %wv.1, ...), custom_call_target="tpu_custom_call" | custom-call | tf_op jit(solution)/shard_map/pallas_call | solution.py:438
  45.6 1.3 %shard_map.222 = (bf16[32,256]{1,0:T(8,128)(2,1)}, f32[32,128,128]{2,1,0:T(8,128)}) custom-call(bf16[32,256]{1,0:T(8,128)(2,1)S(1)} %get-tuple-element.6.result, f32[32,128,128]{2,1,0:T(8,128)S(1)} %get-tuple-element.7.new_state), custom_call_target="tpu_custom_call" | custom-call | tf_op jit(solution)/shard_map/pallas_call | solution.py:448

commit v8 on v7

--- a/solution.py
+++ b/solution.py
@@ -35,10 +35,6 @@
 
 def dot_t(a, b):
     return lax.dot_general(a, b, (((1,), (1,)), ((), ())), preferred_element_type=F32)
-
-
-def t_dot(a, b):
-    return lax.dot_general(a, b, (((0,), (0,)), ((), ())), preferred_element_type=F32)
 
 
 def iota(shape, dim):
@@ -134,8 +130,9 @@
     for h in range(2):
         here = hit & (row % 2 == h)
         send_mat[h, : NEP * 8] = jnp.where(here, 1.0, 0.0).astype(BF16)
-        take_mat[2 * h] = jnp.where(here, coarse, 0.0).astype(BF16)
-        take_mat[2 * h + 1] = jnp.where(here, fine, 0.0).astype(BF16)
+        for i, part in enumerate((coarse, fine)):
+            rows = slice((2 * h + i) * SEQ, (2 * h + i + 1) * SEQ)
+            take_mat[rows] = jnp.where(here, part, 0.0).T.astype(BF16)
     t_row, t_col = iota((NTP * 8, SEQ), 0), iota((NTP * 8, SEQ), 1)
     for h in range(2):
         send_mat[h, NEP * 8 :] = jnp.where((t_row // 2 == t_col) & (t_row % 2 == h), 1.0, 0.0).astype(BF16)
@@ -214,18 +211,24 @@
     moved = (dot(send_mat[0], low) + dot(send_mat[1], high)).reshape(NEP + NTP, 8, 128).astype(BF16)
     disp[...] = moved[:NEP]
     own_tok[...] = moved[NEP:]
-    for dz in FAR_Z + (0,):
+    def dispatch(dz):
         base = z_peer(dz)[0] - x
         for d in (2, 1, 3, 0):
             if dz or d:
                 to = base + lax.rem(x + d, NX)
                 remote(disp.at[to], xa.at[t, ep], d_recv.at[ROUND_OF[dz]], (to, t))
-    xa[t, ep] = disp[ep]
-    for dz in FAR_Z + (0,):
+
+    def tokens(dz):
         for d in FAR_TP + (0,):
             if dz or d:
                 to = lax.rem(t + d, NTP)
                 remote(own_tok.at[to], dx.at[ep, t], t_recv.at[ROUND_OF[dz]], (z_peer(dz)[0], to))
+
+    for dz in FAR_Z + (0,):
+        dispatch(dz)
+    for dz in FAR_Z + (0,):
+        tokens(dz)
+    xa[t, ep] = disp[ep]
     dx[ep, t] = own_tok[t]
     for distance in range(NZ // 2 + 1):
         group = [dz for dz in range(NZ) if ROUND_OF[dz] == distance]
@@ -285,7 +288,7 @@
         square, outs = 0.0, [0.0, 0.0]
         for number, b in enumerate(slots):
             base = pl.multiple_of(b * WIDTH, WIDTH)
-            stage_e[number] = xa[b].astype(F32).reshape(256, 128)
+            stage_e[number, pl.ds(0, 256), :] = xa[b].astype(F32).reshape(256, 128)
             parts = [stage_e[number, pl.ds(h, ROWS, stride=2), :] for h in range(2)]
             square = square + parts[0] * parts[0] + parts[1] * parts[1]
             gain = v_fgain[b]
@@ -325,7 +328,7 @@
         take(pr.at[0], p_recv.at[d])
         qs[there] = (pb[there * 2 + c].astype(F32) + pr[there].astype(F32)).astype(BF16)
         if d > 0:
-            remote(qs.at[there], yr.at[d - 1], q_recv.at[d - 1], y_peer(d))
+            remote(qs.at[there], yr.at[d - 1], q_recv, y_peer(d))
 
     def sum_x(half, f):
         take(xr.at[half, :, f], u_recv.at[half, f])
@@ -359,8 +362,7 @@
     sum_x(1, 2)
     sum_x(1, 3)
     fr[z * NTP + t] = zs[0, t]
-    for d in (1, 3, 2):
-        take(yr.at[0], q_recv.at[d - 1])
+    take(yr, q_recv)
     total = qs[y].astype(F32)
     for d in range(3):
         total = total + yr[d].astype(F32)
@@ -384,9 +386,10 @@
     stage[pl.ds(0, 64), :] = total.reshape(64, 128)
     take(rb.at[pl.ds(0, NEP - 1)], b_recv)
     back = rb[...].astype(F32).reshape(NEP * 8, 128).astype(BF16)
+    taken = dot(take_mat[...], back)
     for h in range(2):
         cols = slice(h * 128, (h + 1) * 128)
-        moe = t_dot(take_mat[2 * h], back) + t_dot(take_mat[2 * h + 1], back)
+        moe = taken[2 * h * SEQ : (2 * h + 1) * SEQ] + taken[(2 * h + 1) * SEQ : (2 * h + 2) * SEQ]
         dense_out = stage[pl.ds(h, SEQ, stride=2), :]
         result[:, cols] = (
             mixed_s[:, cols].astype(F32) + moe + jax.nn.sigmoid(v_mix[:, cols]) * dense_out
@@ -423,14 +426,14 @@
     dma = pltpu.SemaphoreType.DMA
     scratch = vmem_of + [
         V((NTP, SEQ, DK), BF16), V((SEQ, WIDTH), BF16),
-        V((2, (NEP + NTP) * 8, SEQ), BF16), V((4, NEP * 8, SEQ), BF16),
-        V((NEP, 8, 128), BF16), V((NTP, NEP, 8, 128), BF16), V((16 * PITCH, 128), F32), V((3, 256, 128), F32),
+        V((2, (NEP + NTP) * 8, SEQ), BF16), V((4 * SEQ, NEP * 8), BF16),
+        V((NEP, 8, 128), BF16), V((NTP, NEP, 8, 128), BF16), V((18 * PITCH, 128), F32), V((3, 264, 128), F32),
         V((ROWS, 128), F32), V((2, ROWS, FE), F32), V((NTP, ROWS, WIDTH), BF16), V((4, ROWS, WIDTH), BF16), V((4, ROWS, WIDTH), BF16),
         V((3, ROWS, WIDTH), BF16), V((NEP, 8, 128), BF16), V((NEP, 8, 128), BF16),
         V((NTP, 8, 128), BF16), V((NEP, NTP, 8, 128), BF16), V((2, NX * 16, D), F32), V((2, NX * 16, 128), F32),
         V((2, NX, CHUNKS, 16, WIDE), BF16), V((2, NX - 1, CHUNKS, 16, WIDE), BF16), V((16, WIDE), F32),
         V((NZ, NTP, 8, 128), BF16), V((NZ * NTP, 8, 128), BF16), V((SENT, 8, 128), BF16),
-        dma((17,)), dma, dma((2,)), dma, dma((5,)), dma((5,)), dma((2,)), dma((3,)), dma((2,)), dma((4,)), dma((3,)),
+        dma((17,)), dma, dma((2,)), dma, dma((5,)), dma((5,)), dma((2,)), dma((3,)), dma((2,)), dma((4,)), dma,
         dma, dma((2, CHUNKS)), dma,
         pltpu.SemaphoreType.REGULAR((3,)),
     ]

time: 47.1 us -> 47 us (level)
  no operation moved by 1% of the time
where the time goes in v8:
time: 47 us; the launch traced here: 46.8 us
  Pallas kernels  46.2 us (98%)
  between operations  0.65 us (1%)
    pallas_call x1, Pallas kernels, per_device(): pl.pallas_call(kernel, out_shape=kept, in_specs=[pl.BlockSpec(memory_spac...  44.8 us
    pallas_call x1, Pallas kernels, per_device(): pl.pallas_call(write_out, out_shape=tuple((jax.ShapeDtypeStruct(k.shape,...  1.34 us

profile of v8, /device:TPU:1, one launch (start us, length us, event | category | flops | bytes accessed | tf_op | source)
XLA Modules:
  0.0 46.8 jit_solution(15460456974593095339)
XLA Ops:
  0.6 44.8 %shard_map.221 = (bf16[32,256]{1,0:T(8,128)(2,1)S(1)}, f32[32,128,128]{2,1,0:T(8,128)S(1)}) custom-call(bf16[32,256]{1,0:T(8,128)(2,1)} %hidden.1, f32[32,128,128]{2,1,0:T(8,128)} %bitcast.16, f32[8,1,256]{2,1,0:T(1,128)} %bitcast.22, bf16[2048,128]{1,0:T(8,128)(2,1)} %wq.1, bf16[2048,128]{1,0:T(8,128)(2,1)} %wk.1, bf16[2048,128]{1,0:T(8,128)(2,1)} %wv.1, ...), custom_call_target="tpu_custom_call" | custom-call | tf_op jit(solution)/shard_map/pallas_call | solution.py:441
  45.5 1.3 %shard_map.222 = (bf16[32,256]{1,0:T(8,128)(2,1)}, f32[32,128,128]{2,1,0:T(8,128)}) custom-call(bf16[32,256]{1,0:T(8,128)(2,1)S(1)} %get-tuple-element.6.result, f32[32,128,128]{2,1,0:T(8,128)S(1)} %get-tuple-element.7.new_state), custom_call_target="tpu_custom_call" | custom-call | tf_op jit(solution)/shard_map/pallas_call | solution.py:451

commit v9 on v8

--- a/solution.py
+++ b/solution.py
@@ -191,7 +191,7 @@
     read = read * lax.rsqrt(jnp.mean(read * read, axis=-1, keepdims=True) + EPS) * v_hgain[...]
     heads_all[t] = (read * silu(gates)).astype(BF16)
     for d in FAR_TP:
-        remote(heads_all.at[t], heads_all.at[t], h_recv, tp_peer(d))
+        remote(heads_all.at[t], heads_all.at[t], h_recv.at[0 if d in NEAR_TP else 1], tp_peer(d))
     update = beta * (values - decay * s_k)
     keys_t = jnp.concatenate([keys, jnp.zeros((DK - SEQ, DK), F32)], axis=0).T
     decay_rows = jnp.broadcast_to(decay, (SEQ, DK))
@@ -200,10 +200,17 @@
 
     pl.semaphore_wait(met.at[2], 4)
     loads["wo"]()
-    take(heads_all.at[pl.ds(0, 7)], h_recv)
-    wide = hid_all[t].astype(F32)
-    for b in range(NTP):
-        wide = wide + dot(heads_all[b], v_wo[b * DK : (b + 1) * DK, :])
+
+    def project_out(slots):
+        total = 0.0
+        for b in slots:
+            total = total + dot(heads_all[b], v_wo[pl.ds(pl.multiple_of(b * DK, DK), DK), :])
+        return total
+
+    take(heads_all.at[pl.ds(0, 4)], h_recv.at[0])
+    wide = hid_all[t].astype(F32) + project_out([t] + [lax.rem(t + NTP - d, NTP) for d in NEAR_TP])
+    take(heads_all.at[pl.ds(0, 3)], h_recv.at[1])
+    wide = wide + project_out([lax.rem(t + NTP - d, NTP) for d in (3, 5, 4)])
     mixed = wide.astype(BF16)
     mixed_s[...] = mixed
     low, high = mixed[:, :128], mixed[:, 128:]
@@ -433,7 +440,7 @@
         V((NTP, 8, 128), BF16), V((NEP, NTP, 8, 128), BF16), V((2, NX * 16, D), F32), V((2, NX * 16, 128), F32),
         V((2, NX, CHUNKS, 16, WIDE), BF16), V((2, NX - 1, CHUNKS, 16, WIDE), BF16), V((16, WIDE), F32),
         V((NZ, NTP, 8, 128), BF16), V((NZ * NTP, 8, 128), BF16), V((SENT, 8, 128), BF16),
-        dma((17,)), dma, dma((2,)), dma, dma((5,)), dma((5,)), dma((2,)), dma((3,)), dma((2,)), dma((4,)), dma,
+        dma((17,)), dma, dma((2,)), dma((2,)), dma((5,)), dma((5,)), dma((2,)), dma((3,)), dma((2,)), dma((4,)), dma,
         dma, dma((2, CHUNKS)), dma,
         pltpu.SemaphoreType.REGULAR((3,)),
     ]

time: 47 us -> 47 us (level)
  no operation moved by 1% of the time
where the time goes in v9:
time: 47 us; the launch traced here: 46.9 us
  Pallas kernels  46.2 us (98%)
  between operations  0.65 us (1%)
    pallas_call x1, Pallas kernels, per_device(): pl.pallas_call(kernel, out_shape=kept, in_specs=[pl.BlockSpec(memory_spac...  44.9 us
    pallas_call x1, Pallas kernels, per_device(): pl.pallas_call(write_out, out_shape=tuple((jax.ShapeDtypeStruct(k.shape,...  1.34 us

profile of v9, /device:TPU:1, one launch (start us, length us, event | category | flops | bytes accessed | tf_op | source)
XLA Modules:
  0.0 46.9 jit_solution(6108199469009397012)
XLA Ops:
  0.6 44.9 %shard_map.221 = (bf16[32,256]{1,0:T(8,128)(2,1)S(1)}, f32[32,128,128]{2,1,0:T(8,128)S(1)}) custom-call(bf16[32,256]{1,0:T(8,128)(2,1)} %hidden.1, f32[32,128,128]{2,1,0:T(8,128)} %bitcast.16, f32[8,1,256]{2,1,0:T(1,128)} %bitcast.22, bf16[2048,128]{1,0:T(8,128)(2,1)} %wq.1, bf16[2048,128]{1,0:T(8,128)(2,1)} %wk.1, bf16[2048,128]{1,0:T(8,128)(2,1)} %wv.1, ...), custom_call_target="tpu_custom_call" | custom-call | tf_op jit(solution)/shard_map/pallas_call | solution.py:448
  45.5 1.3 %shard_map.222 = (bf16[32,256]{1,0:T(8,128)(2,1)}, f32[32,128,128]{2,1,0:T(8,128)}) custom-call(bf16[32,256]{1,0:T(8,128)(2,1)S(1)} %get-tuple-element.6.result, f32[32,128,128]{2,1,0:T(8,128)S(1)} %get-tuple-element.7.new_state), custom_call_target="tpu_custom_call" | custom-call | tf_op jit(solution)/shard_map/pallas_call | solution.py:458
